TPU v7x, 32 devices: a whole 2x2x4 slice. The times are simulated.
32 devices in a mesh: grp: 2 (over y), sp: 4 (over z), tp: 4 (over x, core).
Axes of the slice: x: 2, y: 2, z: 4, core: 2. Of those that a mesh axis runs over, the one named last changes fastest.
Arguments:
- tokens: bfloat16 [4096, 2048], P(('grp', 'sp')), parts along dimension 0, may hold values from -6 to 6
- gate_in: bfloat16 [2, 2048, 512], P(None, 'sp', 'tp'), may hold values from -0.125 to 0.125
- gate_conv: bfloat16 [2, 2048, 512], P(None, 'sp', 'tp'), may hold values from -0.125 to 0.125
- value_in: bfloat16 [2, 2048, 512], P(None, 'sp', 'tp'), may hold values from -0.125 to 0.125
- out_weight: bfloat16 [2, 512, 2048], P(None, None, 'sp'), may hold values from -0.25 to 0.25
- conv_taps: float32 [2, 3, 512], replicated, may hold values from -7 to 7
- pre_gain: float32 [2, 2048], replicated, may hold values from 0.1 to 1.9
- mix_gain: float32 [2, 512], replicated, may hold values from 0.1 to 1.9
- post_gain: float32 [2, 2048], replicated, may hold values from 0.1 to 1.9
Outputs:
- result: bfloat16 [4096, 2048], P(('grp', 'sp', 'tp')), parts along dimension 0
There are 2 independent parts, one for each index of `grp`. A program takes and returns all parts, laid end to end along the dimension named above; an argument that names none is the same for every part. Nothing has to cross between parts.
All inputs are finite; a program needn't handle non-finite values.
Results may differ from a plain program's by a relative error of at most 0.011.
Values may be sent and summed in bfloat16 or wider, within the bound.
A program may use at most 64 MiB of HBM per device.

v0:
```python
import functools

import jax
import jax.numpy as jnp
from jax import lax
from jax.experimental import pallas as pl
from jax.experimental.pallas import tpu as pltpu
from jax.sharding import PartitionSpec as P

EPS = 1e-06


def passed_along(x, axis, by):
    length = lax.axis_size(axis)
    pairs = [(i, i + by) for i in range(length) if 0 <= i + by < length]
    return lax.ppermute(x, axis, pairs)


def rms_norm(values, gain):
    return values * lax.rsqrt(jnp.mean(values * values, axis=-1, keepdims=True) + EPS) * gain


def stored(values):
    return lax.optimization_barrier(values.astype(jnp.bfloat16))


def per_device(
    tokens, gate_in, gate_conv, value_in, out_weight, conv_taps, pre_gain, mix_gain, post_gain
):
    layer_count = gate_in.shape[0]
    channel_count = gate_in.shape[2]
    tap_count = conv_taps.shape[1]
    row_count = tokens.shape[0]
    tp_size = lax.axis_size("tp")
    tp_index = lax.axis_index("tp")
    row_share = row_count // tp_size
    stream = tokens.astype(jnp.float32)
    for layer_index in range(layer_count):
        is_last = layer_index == layer_count - 1
        normed = stored(rms_norm(stream, pre_gain[layer_index]))
        outer_whole, inner_whole, value_whole = (
            lax.all_gather(gate_in[layer_index], "sp", axis=0, tiled=True),
            lax.all_gather(gate_conv[layer_index], "sp", axis=0, tiled=True),
            lax.all_gather(value_in[layer_index], "sp", axis=0, tiled=True),
        )
        out_whole = lax.all_gather(out_weight[layer_index], "sp", axis=1, tiled=True)
        outer = stored(jnp.dot(normed, outer_whole, preferred_element_type=jnp.float32))
        inner = stored(jnp.dot(normed, inner_whole, preferred_element_type=jnp.float32))
        values = stored(jnp.dot(normed, value_whole, preferred_element_type=jnp.float32))
        gated = stored(inner.astype(jnp.float32) * values.astype(jnp.float32))
        before = passed_along(gated[row_count - (tap_count - 1) :], "sp", 1)
        padded = jnp.concatenate([before, gated], axis=0)
        taps_here = lax.dynamic_slice_in_dim(
            conv_taps[layer_index], tp_index * channel_count, channel_count, 1
        )
        filtered = jnp.zeros((row_count, channel_count), jnp.float32)
        for tap_index in range(tap_count):
            filtered = filtered + taps_here[tap_index] * padded[
                tap_index : tap_index + row_count
            ].astype(jnp.float32)
        mixed_raw = stored(outer.astype(jnp.float32) * filtered)
        if is_last:
            arrived = lax.all_to_all(mixed_raw, "tp", split_axis=0, concat_axis=1, tiled=True)
            residual = lax.dynamic_slice_in_dim(stream, tp_index * row_share, row_share, 0)
        else:
            arrived = lax.all_gather(mixed_raw, "tp", axis=1, tiled=True)
            residual = stream
        mixed = stored(rms_norm(arrived.astype(jnp.float32), mix_gain[layer_index]))
        branch = stored(jnp.dot(mixed, out_whole, preferred_element_type=jnp.float32))
        stream = residual + rms_norm(branch.astype(jnp.float32), post_gain[layer_index])
    return stream.astype(jnp.bfloat16)


MESH = pl.DeviceIdType.MESH


def fused_kernel(
    sizes,
    tok_hbm, gate_hbm, conv_hbm, value_hbm, outw_hbm, taps_hbm, pre_hbm, mixg_hbm, post_hbm,
    out_ref, taps_ref, pre_ref, mixg_ref, post_ref,
    tok, nrm, w, ow, gpad, outer, halo_tx, halo_rx, m, ms, mlast, mx, br, res,
    loc, zsw, zrw, zso, zro, ysw, yrw, yso, yro, xso, xro, cso, cro, hs, hr_sem, ts, tr, a2s, a2r, small,
):
    layers, grp, sp, tp, ch, rows, depth, cols = sizes
    width = sp * cols
    taps = taps_ref.shape[1]
    g = lax.axis_index("grp")
    s = lax.axis_index("sp")
    t = lax.axis_index("tp")
    x = t // 2
    c = t % 2
    sibling = x * 2 + (1 - c)
    across = (1 - x) * 2 + c
    diagonal = (1 - x) * 2 + (1 - c)
    share = rows // tp
    half = depth // 2
    part = (tp * ch) // (2 * tp)
    pending = []

    def when(cond, body):
        if cond is None:
            body()
        else:
            pl.when(cond)(body)

    def copy(ref_from, ref_to, send, recv, **device):
        return pltpu.make_async_remote_copy(
            src_ref=ref_from, dst_ref=ref_to, send_sem=send, recv_sem=recv,
            device_id=device, device_id_type=MESH,
        )

    def start(cond, make):
        when(cond, lambda: make().start())
        pending.append((cond, make))

    piece_rows = half // PIECES

    def w_half(l, j, h, p):
        first = pl.multiple_of(h * half + p * piece_rows, piece_rows)
        return w.at[l, j, pl.ds(first, piece_rows), :]

    def o_rows(l, j, first, count):
        return ow.at[l, j, pl.ds(pl.multiple_of(first, part), count), :]

    my_part = ((c * 2 + x) * 2 + g) * part
    your_part = ((c * 2 + x) * 2 + (1 - g)) * part

    def z_w(l, j, way, p):
        r = w_half(l, j, g, p)
        return copy(r, r, zsw.at[l, (way + 1) // 2, j, p], zrw.at[l, j, p], sp=s + way)

    def z_o(l, j, way):
        r = o_rows(l, j, my_part, part)
        return copy(r, r, zso.at[l, (way + 1) // 2, j], zro.at[l, j], sp=s + way)

    def y_w(l, j, h, p):
        r = w_half(l, j, h, p)
        return copy(r, r, ysw.at[l, j, p], yrw.at[l, j, p], grp=1 - g)

    def y_o(l, j, first):
        r = o_rows(l, j, first, part)
        return copy(r, r, yso.at[l, j], yro.at[l, j], grp=1 - g)

    def x_o(l, j, side):
        r = o_rows(l, j, (c * 2 + side) * 2 * part, 2 * part)
        return copy(r, r, xso.at[l, j], xro.at[l, j], tp=across)

    def c_o(l, j, core):
        r = o_rows(l, j, core * 4 * part, 4 * part)
        return copy(r, r, cso.at[l, j], cro.at[l, j], tp=sibling)

    def sides(k):
        return ((s >= k, s - k, 1, s < sp - 1), (s + k < sp, s + k, -1, s > 0))

    def both(*conds):
        value = conds[0]
        for cond in conds[1:]:
            value = jnp.logical_and(value, cond)
        return value

    def own_to(l, way, cond):
        for p in range(PIECES):
            start(cond, lambda p=p: z_w(l, s, way, p))
        start(cond, lambda: z_o(l, s, way))

    def own_after(l, k):
        if l >= layers:
            return
        if k == 0:
            when(None, lambda: wait_local(l))
        own_to(l, 1, both(s == k, s < sp - 1))
        own_to(l, -1, both(sp - 1 - s == k, s > 0))

    def fwd(l, k):
        for has, j, way, more in sides(k):
            cond = both(has, more)
            for p in range(PIECES):
                when(cond, lambda: z_w(l, j, way, p).wait_recv())
                start(cond, lambda l=l, j=j, way=way, p=p: z_w(l, j, way, p))
                start(cond, lambda l=l, j=j, p=p: y_w(l, j, g, p))
            when(cond, lambda: z_o(l, j, way).wait_recv())
            start(cond, lambda l=l, j=j, way=way: z_o(l, j, way))
            start(cond, lambda l=l, j=j: y_o(l, j, my_part))

    def end_w(l, k):
        for has, j, way, more in sides(k):
            cond = both(has, jnp.logical_not(more))
            for p in range(PIECES):
                when(cond, lambda: z_w(l, j, way, p).wait_recv())
                start(cond, lambda l=l, j=j, p=p: y_w(l, j, g, p))

    def end_o(l, k):
        for has, j, way, more in sides(k):
            cond = both(has, jnp.logical_not(more))
            when(cond, lambda: z_o(l, j, way).wait_recv())
            start(cond, lambda l=l, j=j: y_o(l, j, my_part))

    def y_wait(l, k):
        for has, j, _, _ in sides(k):
            for p in range(PIECES):
                when(has, lambda: y_w(l, j, 1 - g, p).wait_recv())

    def x_phase(l, k):
        for has, j, _, _ in sides(k):
            when(has, lambda: y_o(l, j, your_part).wait_recv())
            start(has, lambda l=l, j=j: x_o(l, j, x))

    def c_phase(l, k):
        for has, j, _, _ in sides(k):
            when(has, lambda: x_o(l, j, 1 - x).wait_recv())
            start(has, lambda l=l, j=j: c_o(l, j, c))

    def c_wait(l, k):
        for has, j, _, _ in sides(k):
            when(has, lambda: c_o(l, j, 1 - c).wait_recv())

    def local_weights(l):
        made = [
            pltpu.make_async_copy(src.at[l], w.at[l, s, :, pl.ds(i * ch, ch)], loc.at[l, i])
            for i, src in enumerate((gate_hbm, conv_hbm, value_hbm))
        ]
        return made + [pltpu.make_async_copy(outw_hbm.at[l], ow.at[l, s], loc.at[l, 3])]

    def wait_local(l):
        for one in local_weights(l):
            one.wait()

    tok_copy = pltpu.make_async_copy(tok_hbm, tok, loc.at[layers, 0])
    small_copies = [
        pltpu.make_async_copy(src, dst, small.at[i])
        for i, (src, dst) in enumerate(
            ((taps_hbm, taps_ref), (pre_hbm, pre_ref), (mixg_hbm, mixg_ref), (post_hbm, post_ref))
        )
    ]
    for l in range(layers):
        for one in local_weights(l):
            one.start()
        if l == 0:
            tok_copy.start()
            for one in small_copies:
                one.start()

    barrier = pltpu.get_barrier_semaphore()

    def greet(**device):
        pl.semaphore_signal(barrier, inc=1, device_id=device, device_id_type=MESH)

    pl.when(s > 0)(lambda: greet(sp=s - 1))
    pl.when(s < sp - 1)(lambda: greet(sp=s + 1))
    greet(grp=1 - g)
    greet(tp=sibling)
    greet(tp=across)
    greet(tp=diagonal)
    at_end = jnp.logical_or(s == 0, s == sp - 1)
    pl.semaphore_wait(barrier, jnp.where(at_end, 5, 6))

    wait_local(0)
    own_to(0, 1, s < sp - 1)
    own_to(0, -1, s > 0)
    own_after(1, 0)

    block = VPU_ROWS
    tok_copy.wait()
    for one in small_copies:
        one.wait()

    def first_norm(i, carry):
        at = pl.ds(pl.multiple_of(i * block, block), block)
        v = tok[at, :].astype(jnp.float32)
        scale = lax.rsqrt(jnp.sum(v * v, axis=-1, keepdims=True) * (1.0 / width) + EPS)
        nrm[at, :] = (v * scale * pre_ref[0:1, :]).astype(jnp.bfloat16)
        return carry

    lax.fori_loop(0, rows // block, first_norm, 0)

    for k in range(1, sp):
        fwd(0, k)
        end_w(0, k)
        end_o(0, k)
        own_after(1, k)
        if k > 1:
            x_phase(0, k - 1)

    def halo(l):
        return copy(halo_tx.at[l], halo_rx.at[l], hs.at[l], hr_sem.at[l], sp=s + 1)

    hrows = halo_tx.shape[1]
    big = rows // 2

    for l in range(layers):
        last = l == layers - 1
        if not last:
            fwd(l + 1, 1)
        for k in range(1, sp):
            y_wait(l, k)
        if not last:
            end_w(l + 1, 1)
            end_o(l + 1, 1)
        for piece in reversed(range(rows // big)):
            at = pl.ds(piece * big, big)
            prod = jnp.dot(
                nrm[at, :], w[l].reshape(sp * depth, 3 * ch), preferred_element_type=jnp.float32
            ).astype(jnp.bfloat16)
            outer[at, :] = prod[:, :ch]
            gated = (
                prod[:, ch : 2 * ch].astype(jnp.float32) * prod[:, 2 * ch :].astype(jnp.float32)
            ).astype(jnp.bfloat16)
            gpad[pl.ds(8 + piece * big, big), :] = gated.astype(jnp.float32)
            if piece == rows // big - 1:
                halo_tx[l] = gated[big - hrows :, :]
                start(s < sp - 1, lambda l=l: halo(l))
        if last:
            x_phase(l, sp - 1)
        for piece in reversed(range(tp)):
            if piece == 0:
                @pl.when(s == 0)
                def _():
                    gpad[0:8, :] = jnp.zeros((8, ch), jnp.float32)

                @pl.when(s > 0)
                def _():
                    halo(l).wait_recv()
                    gpad[0:8, :] = halo_rx[l].astype(jnp.float32)[hrows - 8 :, :]
            at = pl.ds(piece * share, share)
            filtered = jnp.zeros((share, ch), jnp.float32)
            for k in range(taps):
                tap = taps_ref[l, k : k + 1, pl.ds(pl.multiple_of(t * ch, ch), ch)]
                filtered = filtered + tap * gpad[pl.ds(8 - (taps - 1) + k + piece * share, share), :]
            raw = (outer[at, :].astype(jnp.float32) * filtered).astype(jnp.bfloat16)
            if last:
                ms[at, :] = raw

                @pl.when(t == piece)
                def _():
                    mlast[t] = raw

                start(t != piece, lambda at=at, piece=piece: copy(
                    ms.at[at, :], mlast.at[t], a2s.at[piece], a2r.at[t], tp=piece))
            else:
                m[l, t, at, :] = raw

                def tp_copy(l, j, at, piece, kind, to):
                    r = m.at[l, j, at, :]
                    return copy(r, r, ts.at[l, kind, piece], tr.at[l, j, piece], tp=to)

                start(None, lambda l=l, at=at, piece=piece: tp_copy(l, t, at, piece, 0, across))
                start(None, lambda l=l, at=at, piece=piece: tp_copy(l, t, at, piece, 1, sibling))

        if not last:
            x_phase(l, sp - 1)
            for k in range(2, sp - 1):
                fwd(l + 1, k)
                end_w(l + 1, k)
                end_o(l + 1, k)
            for piece in reversed(range(tp)):
                at = pl.ds(piece * share, share)
                tp_copy(l, across, at, piece, 0, across).wait_recv()
                start(None, lambda l=l, at=at, piece=piece: tp_copy(l, across, at, piece, 2, sibling))
            for k in range(1, sp):
                c_phase(l, k)
            x_phase(l + 1, 1)
            for piece in range(tp):
                at = pl.ds(piece * share, share)
                tp_copy(l, sibling, at, piece, 1, sibling).wait_recv()
                tp_copy(l, diagonal, at, piece, 2, sibling).wait_recv()
        else:
            for k in range(2, sp):
                c_phase(l, k)
            for piece in range(tp):
                @pl.when(t != piece)
                def _():
                    copy(ms.at[pl.ds(0, share), :], mlast.at[piece], a2s.at[piece], a2r.at[piece], tp=piece).wait_recv()

        def mix(read):
            parts = [read(j).astype(jnp.float32) for j in range(tp)]
            total = parts[0] * parts[0]
            for one in parts[1:]:
                total = total + one * one
            scale = lax.rsqrt(jnp.sum(total, axis=-1, keepdims=True) * (1.0 / (tp * ch)) + EPS)
            return [
                (one * scale * mixg_ref[l : l + 1, j * ch : (j + 1) * ch]).astype(jnp.bfloat16)
                for j, one in enumerate(parts)
            ]

        def project(mixed):
            count = mixed.shape[0]
            for j in range(sp):
                br[pl.ds(0, count), j * cols : (j + 1) * cols] = jnp.dot(
                    mixed, ow[l, j], preferred_element_type=jnp.float32
                ).astype(jnp.bfloat16).astype(jnp.float32)

        for k in range(1, sp):
            c_wait(l, k)
        if last:
            mixed = jnp.concatenate(mix(lambda j: mlast[j]), axis=1)
            project(mixed)

            def last_rows(i, carry):
                at = pl.ds(pl.multiple_of(i * block, block), block)
                b = br[at, :]
                scale = lax.rsqrt(jnp.sum(b * b, axis=-1, keepdims=True) * (1.0 / width) + EPS)
                if layers > 1:
                    base = res[at, :]
                else:
                    base = tok[pl.ds(pl.multiple_of(t * share + i * block, block), block), :].astype(jnp.float32)
                out_ref[at, :] = (base + b * scale * post_ref[l : l + 1, :]).astype(jnp.bfloat16)
                return carry

            lax.fori_loop(0, share // block, last_rows, 0)
        else:
            for piece in range(rows // big):
                at = pl.ds(piece * big, big)
                mixed = jnp.concatenate(mix(lambda j: m[l, j, at, :]), axis=1)
                project(mixed)

                def next_rows(i, carry):
                    inside = pl.ds(pl.multiple_of(i * block, block), block)
                    first = piece * big + i * block
                    whole = pl.ds(pl.multiple_of(first, block), block)
                    b = br[inside, :]
                    scale = lax.rsqrt(jnp.sum(b * b, axis=-1, keepdims=True) * (1.0 / width) + EPS)
                    v = tok[whole, :].astype(jnp.float32) + b * scale * post_ref[l : l + 1, :]

                    @pl.when(first // share == t)
                    def _():
                        res[pl.ds(pl.multiple_of(first - t * share, block), block), :] = v

                    scale = lax.rsqrt(jnp.sum(v * v, axis=-1, keepdims=True) * (1.0 / width) + EPS)
                    nrm[whole, :] = (v * scale * pre_ref[l + 1 : l + 2, :]).astype(jnp.bfloat16)
                    return carry

                lax.fori_loop(0, big // block, next_rows, 0)
            end_w(l + 1, sp - 1)
            end_o(l + 1, sp - 1)
            for k in range(2, sp - 1):
                x_phase(l + 1, k)
            c_phase(l + 1, 1)

    for cond, make in pending:
        when(cond, lambda: make().wait_send())


VPU_ROWS = 64
PIECES = 2
VMEM_GRANT = 63 * 1024 * 1024


def fused(sizes, tokens, gate_in, gate_conv, value_in, out_weight, conv_taps, pre_gain, mix_gain, post_gain):
    layers, grp, sp, tp, ch, rows, depth, cols = sizes
    width = sp * cols
    share = rows // tp
    bf, f32 = jnp.bfloat16, jnp.float32
    dma = pltpu.SemaphoreType.DMA
    hbm = pl.BlockSpec(memory_space=pltpu.HBM)
    vmem = pl.BlockSpec(memory_space=pltpu.VMEM)
    return pl.pallas_call(
        functools.partial(fused_kernel, sizes),
        out_shape=jax.ShapeDtypeStruct((share, width), bf),
        in_specs=[hbm] * 9,
        out_specs=vmem,
        scratch_shapes=[
            pltpu.VMEM(conv_taps.shape, f32),
            pltpu.VMEM(pre_gain.shape, f32),
            pltpu.VMEM(mix_gain.shape, f32),
            pltpu.VMEM(post_gain.shape, f32),
            pltpu.VMEM((rows, width), bf),
            pltpu.VMEM((rows, width), bf),
            pltpu.VMEM((layers, sp, depth, 3 * ch), bf),
            pltpu.VMEM((layers, sp, tp * ch, cols), bf),
            pltpu.VMEM((8 + rows, ch), f32),
            pltpu.VMEM((rows, ch), bf),
            pltpu.VMEM((layers, 16, ch), bf),
            pltpu.VMEM((layers, 16, ch), bf),
            pltpu.VMEM((max(layers - 1, 1), tp, rows, ch), bf),
            pltpu.VMEM((rows, ch), bf),
            pltpu.VMEM((tp, share, ch), bf),
            pltpu.VMEM((16, 128), bf),
            pltpu.VMEM((rows // 2, width), f32),
            pltpu.VMEM((share, width), f32),
            dma((layers + 1, 4)),
            dma((layers, 2, sp, PIECES)), dma((layers, sp, PIECES)),
            dma((layers, 2, sp)), dma((layers, sp)),
            dma((layers, sp, PIECES)), dma((layers, sp, PIECES)),
            dma((layers, sp)), dma((layers, sp)),
            dma((layers, sp)), dma((layers, sp)),
            dma((layers, sp)), dma((layers, sp)),
            dma((layers,)), dma((layers,)),
            dma((max(layers - 1, 1), 3, tp)), dma((max(layers - 1, 1), tp, tp)),
            dma((tp,)), dma((tp,)), dma((4,)),
        ],
        compiler_params=pltpu.CompilerParams(
            collective_id=0, has_side_effects=True, vmem_limit_bytes=VMEM_GRANT
        ),
    )(tokens, gate_in, gate_conv, value_in, out_weight, conv_taps, pre_gain, mix_gain, post_gain)


def fits(sizes, taps):
    layers, grp, sp, tp, ch, rows, depth, cols = sizes
    width = sp * cols
    share = rows // tp
    held = rows * width * 4 + layers * sp * depth * 6 * ch + layers * tp * ch * width * 2
    held += rows * width * 2 + share * width * 8 + layers * tp * rows * ch * 2
    return (
        grp == 2 and tp == 4 and 3 <= sp <= 8 and layers == 2 and taps <= 9
        and ch % 128 == 0 and cols % 128 == 0 and rows % 512 == 0 and depth % 256 == 0
        and held < 40 * 1024 * 1024
    )


def chosen(*arrays):
    tokens, gate_in, _, _, out_weight, conv_taps = arrays[:6]
    sizes = (
        gate_in.shape[0], lax.axis_size("grp"), lax.axis_size("sp"), lax.axis_size("tp"),
        gate_in.shape[2], tokens.shape[0], gate_in.shape[1], out_weight.shape[2],
    )
    if fits(sizes, conv_taps.shape[1]):
        return fused(sizes, *arrays)
    return per_device(*arrays)


def solution(mesh):
    placed = (
        P(("grp", "sp"), None),
        P(None, "sp", "tp"),
        P(None, "sp", "tp"),
        P(None, "sp", "tp"),
        P(None, None, "sp"),
        P(),
        P(),
        P(),
        P(),
    )
    return jax.shard_map(
        chosen,
        mesh=mesh,
        in_specs=placed,
        out_specs=P(("grp", "sp", "tp"), None),
        check_vma=False,
    )
```

profile of v0, /device:TPU:0, one launch (start us, length us, event | category | flops | bytes accessed | tf_op | source)
XLA Modules:
  0.0 65.3 jit_solution(15548974743139537894)
XLA Ops:
  0.0 1.3 %copy.10.taps_hbm = f32[2,3,512]{2,1,0:T(4,128)} copy(f32[2,3,512]{2,0,1:T(2,128)} %param.14) | data formatting | bytes 24576 | tf_op args[5]
  1.3 62.1 %shard_map.91 = bf16[128,2048]{1,0:T(8,128)(2,1)} custom-call(bf16[512,2048]{1,0:T(8,128)(2,1)} %tok_hbm.1, bf16[2,512,128]{2,1,0:T(8,128)(2,1)} %gate_hbm.1, bf16[2,512,128]{2,1,0:T(8,128)(2,1)} %conv_hbm.1, bf16[2,512,128]{2,1,0:T(8,128)(2,1)} %value_hbm.1, bf16[2,512,512]{2,1,0:T(8,128)(2,1)} %outw_hbm.1, f32[2,3,512]{2,1,0:T(4,128)} %copy.10.taps_hbm, ...), custom_call_target="tpu_custom_call" | custom-call | tf_op jit(solution)/shard_map/pallas_call | solution.py:456
  63.5 1.9 %copy.12 = bf16[128,2048]{1,0:T(8,128)(2,1)} copy(bf16[128,2048]{1,0:T(8,128)(2,1)} %shard_map.91) | data formatting | bytes 1048576
where the time goes:
time: 65.6 us; the launch traced here: 65.3 us
  Pallas kernels  62.1 us (95%)
  local copies, waits for them, and re-layouts  3.2 us (5%)
    pallas_call x1, Pallas kernels, fused(): pl.pallas_call(functools.partial(fused_kernel, sizes), out_shape=jax.Shap...  62.1 us
    unnamed x2, local copies, waits for them, and re-layouts  3.2 us

commit v1 on v0

--- a/solution.py
+++ b/solution.py
@@ -83,7 +83,7 @@
 ):
     layers, grp, sp, tp, ch, rows, depth, cols = sizes
     width = sp * cols
-    taps = taps_ref.shape[1]
+    taps = taps_ref.shape[0]
     g = lax.axis_index("grp")
     s = lax.axis_index("sp")
     t = lax.axis_index("tp")
@@ -324,7 +324,7 @@
             at = pl.ds(piece * share, share)
             filtered = jnp.zeros((share, ch), jnp.float32)
             for k in range(taps):
-                tap = taps_ref[l, k : k + 1, pl.ds(pl.multiple_of(t * ch, ch), ch)]
+                tap = taps_ref[k, l : l + 1, pl.ds(pl.multiple_of(t * ch, ch), ch)]
                 filtered = filtered + tap * gpad[pl.ds(8 - (taps - 1) + k + piece * share, share), :]
             raw = (outer[at, :].astype(jnp.float32) * filtered).astype(jnp.bfloat16)
             if last:
@@ -453,13 +453,14 @@
     dma = pltpu.SemaphoreType.DMA
     hbm = pl.BlockSpec(memory_space=pltpu.HBM)
     vmem = pl.BlockSpec(memory_space=pltpu.VMEM)
-    return pl.pallas_call(
+    taps = jnp.transpose(conv_taps, (1, 0, 2))
+    held = pl.pallas_call(
         functools.partial(fused_kernel, sizes),
-        out_shape=jax.ShapeDtypeStruct((share, width), bf),
+        out_shape=pltpu.VMEM((share, width), bf),
         in_specs=[hbm] * 9,
         out_specs=vmem,
         scratch_shapes=[
-            pltpu.VMEM(conv_taps.shape, f32),
+            pltpu.VMEM(taps.shape, f32),
             pltpu.VMEM(pre_gain.shape, f32),
             pltpu.VMEM(mix_gain.shape, f32),
             pltpu.VMEM(post_gain.shape, f32),
@@ -491,7 +492,8 @@
         compiler_params=pltpu.CompilerParams(
             collective_id=0, has_side_effects=True, vmem_limit_bytes=VMEM_GRANT
         ),
-    )(tokens, gate_in, gate_conv, value_in, out_weight, conv_taps, pre_gain, mix_gain, post_gain)
+    )(tokens, gate_in, gate_conv, value_in, out_weight, taps, pre_gain, mix_gain, post_gain)
+    return held
 
 
 def fits(sizes, taps):

time: 65.6 us -> 62.3 us (0.950)
  local copies, waits for them, and re-layouts: 3.2 us -> 0.8 us
  Pallas kernels: 62.1 us -> 61.3 us
    unnamed x2 -> x1, local copies, waits for them, and re-layouts: 3.2 us -> 0.8 us
    pallas_call x1, Pallas kernels: 62.1 us -> 61.3 us  [fused(): pl.pallas_call(functools.partial(fused_kernel, sizes), out_shape=pltpu.VM...]
where the time goes in v1:
time: 62.3 us; the launch traced here: 62.1 us
  Pallas kernels  61.3 us (98%)
  local copies, waits for them, and re-layouts  0.8 us (1%)
    pallas_call x1, Pallas kernels, fused(): pl.pallas_call(functools.partial(fused_kernel, sizes), out_shape=pltpu.VM...  61.3 us

profile of v1, /device:TPU:0, one launch (start us, length us, event | category | flops | bytes accessed | tf_op | source)
XLA Modules:
  0.0 62.1 jit_solution(4451174337571005599)
XLA Ops:
  0.0 61.3 %shard_map.91 = bf16[128,2048]{1,0:T(8,128)(2,1)S(1)} custom-call(bf16[512,2048]{1,0:T(8,128)(2,1)} %tok_hbm.1, bf16[2,512,128]{2,1,0:T(8,128)(2,1)} %gate_hbm.1, bf16[2,512,128]{2,1,0:T(8,128)(2,1)} %conv_hbm.1, bf16[2,512,128]{2,1,0:T(8,128)(2,1)} %value_hbm.1, bf16[2,512,512]{2,1,0:T(8,128)(2,1)} %outw_hbm.1, f32[3,2,512]{2,1,0:T(2,128)} %bitcast.1, ...), custom_call_target="tpu_custom_call" | custom-call | tf_op jit(solution)/shard_map/pallas_call | solution.py:457
  61.3 0.8 %copy.11 = bf16[128,2048]{1,0:T(8,128)(2,1)} copy(bf16[128,2048]{1,0:T(8,128)(2,1)S(1)} %shard_map.91) | data formatting | bytes 1048576

commit v2 on v1

v2 whole, which is shorter than its diff:
```python
import functools

import jax
import jax.numpy as jnp
from jax import lax
from jax.experimental import pallas as pl
from jax.experimental.pallas import tpu as pltpu
from jax.sharding import PartitionSpec as P

EPS = 1e-06


def passed_along(x, axis, by):
    length = lax.axis_size(axis)
    pairs = [(i, i + by) for i in range(length) if 0 <= i + by < length]
    return lax.ppermute(x, axis, pairs)


def rms_norm(values, gain):
    return values * lax.rsqrt(jnp.mean(values * values, axis=-1, keepdims=True) + EPS) * gain


def stored(values):
    return lax.optimization_barrier(values.astype(jnp.bfloat16))


def per_device(
    tokens, gate_in, gate_conv, value_in, out_weight, conv_taps, pre_gain, mix_gain, post_gain
):
    layer_count = gate_in.shape[0]
    channel_count = gate_in.shape[2]
    tap_count = conv_taps.shape[1]
    row_count = tokens.shape[0]
    tp_size = lax.axis_size("tp")
    tp_index = lax.axis_index("tp")
    row_share = row_count // tp_size
    stream = tokens.astype(jnp.float32)
    for layer_index in range(layer_count):
        is_last = layer_index == layer_count - 1
        normed = stored(rms_norm(stream, pre_gain[layer_index]))
        outer_whole, inner_whole, value_whole = (
            lax.all_gather(gate_in[layer_index], "sp", axis=0, tiled=True),
            lax.all_gather(gate_conv[layer_index], "sp", axis=0, tiled=True),
            lax.all_gather(value_in[layer_index], "sp", axis=0, tiled=True),
        )
        out_whole = lax.all_gather(out_weight[layer_index], "sp", axis=1, tiled=True)
        outer = stored(jnp.dot(normed, outer_whole, preferred_element_type=jnp.float32))
        inner = stored(jnp.dot(normed, inner_whole, preferred_element_type=jnp.float32))
        values = stored(jnp.dot(normed, value_whole, preferred_element_type=jnp.float32))
        gated = stored(inner.astype(jnp.float32) * values.astype(jnp.float32))
        before = passed_along(gated[row_count - (tap_count - 1) :], "sp", 1)
        padded = jnp.concatenate([before, gated], axis=0)
        taps_here = lax.dynamic_slice_in_dim(
            conv_taps[layer_index], tp_index * channel_count, channel_count, 1
        )
        filtered = jnp.zeros((row_count, channel_count), jnp.float32)
        for tap_index in range(tap_count):
            filtered = filtered + taps_here[tap_index] * padded[
                tap_index : tap_index + row_count
            ].astype(jnp.float32)
        mixed_raw = stored(outer.astype(jnp.float32) * filtered)
        if is_last:
            arrived = lax.all_to_all(mixed_raw, "tp", split_axis=0, concat_axis=1, tiled=True)
            residual = lax.dynamic_slice_in_dim(stream, tp_index * row_share, row_share, 0)
        else:
            arrived = lax.all_gather(mixed_raw, "tp", axis=1, tiled=True)
            residual = stream
        mixed = stored(rms_norm(arrived.astype(jnp.float32), mix_gain[layer_index]))
        branch = stored(jnp.dot(mixed, out_whole, preferred_element_type=jnp.float32))
        stream = residual + rms_norm(branch.astype(jnp.float32), post_gain[layer_index])
    return stream.astype(jnp.bfloat16)


MESH = pl.DeviceIdType.MESH


def fused_kernel(
    sizes,
    tok_hbm, gate_hbm, conv_hbm, value_hbm, outw_hbm, taps_hbm, pre_hbm, mixg_hbm, post_hbm,
    out_ref, taps_ref, pre_ref, mixg_ref, post_ref,
    tok, nrm, w, ow, gpad, outer, acc, halo_tx, halo_rx, m, ms, mlast, br, res,
    loc, zsw, zrw, zso, zro, ysw, yrw, yso, yro, xsa, xra, xsb, xrb, csa, cra, dso, dro, csb, crb, hs, hr_sem, ts, tr, a2s, a2r, small,
):
    layers, grp, sp, tp, ch, rows, depth, cols = sizes
    width = sp * cols
    taps = taps_ref.shape[0]
    g = lax.axis_index("grp")
    s = lax.axis_index("sp")
    t = lax.axis_index("tp")
    x = t // 2
    c = t % 2
    sibling = x * 2 + (1 - c)
    across = (1 - x) * 2 + c
    diagonal = (1 - x) * 2 + (1 - c)
    share = rows // tp
    half = depth // 2
    part = (tp * ch) // (2 * tp)
    pending = []

    def when(cond, body):
        if cond is None:
            body()
        else:
            pl.when(cond)(body)

    def both(one, other):
        return other if one is None else jnp.logical_and(one, other)

    def copy(ref_from, ref_to, send, recv, **device):
        return pltpu.make_async_remote_copy(
            src_ref=ref_from, dst_ref=ref_to, send_sem=send, recv_sem=recv,
            device_id=device, device_id_type=MESH,
        )

    def start(cond, make):
        when(cond, lambda: make().start())
        pending.append((cond, make))

    def flush(count=None):
        count = len(pending) if count is None else count
        for cond, make in pending[:count]:
            when(cond, lambda: make().wait_send())
        del pending[:count]

    piece_rows = half // PIECES

    def w_half(l, j, h, p):
        first = pl.multiple_of(h * half + p * piece_rows, piece_rows)
        return w.at[l, j, pl.ds(first, piece_rows), :]

    def o_rows(l, j, first, count):
        return ow.at[l, j, pl.ds(pl.multiple_of(first, part), count), :]

    def o_part(side, group):
        return ((c * 2 + side) * 2 + group) * part

    def z_w(l, j, way, p):
        r = w_half(l, j, g, p)
        return copy(r, r, zsw.at[l, (way + 1) // 2, j, p], zrw.at[l, j, p], sp=s + way)

    def z_o(l, j, way):
        r = o_rows(l, j, o_part(x, g), part)
        return copy(r, r, zso.at[l, (way + 1) // 2, j], zro.at[l, j], sp=s + way)

    def y_w(l, j, h, p):
        r = w_half(l, j, h, p)
        return copy(r, r, ysw.at[l, j, p], yrw.at[l, j, p], grp=1 - g)

    def y_o(l, j, group):
        r = o_rows(l, j, o_part(x, group), part)
        return copy(r, r, yso.at[l, j], yro.at[l, j], grp=1 - g)

    def x_a(l, j, side):
        r = o_rows(l, j, o_part(side, g), part)
        return copy(r, r, xsa.at[l, j], xra.at[l, j], tp=across)

    def x_b(l, j, side):
        r = o_rows(l, j, o_part(side, 1 - g), part)
        return copy(r, r, xsb.at[l, j], xrb.at[l, j], tp=across)

    def d_o(side, group):
        l, j = layers - 1, slice_at(sp - 1)
        r = o_rows(l, j, o_part(side, group), part)
        return copy(r, r, dso.at[0], dro.at[0], tp=across, grp=1 - g)

    def c_a(l, j, core):
        r = o_rows(l, j, (core * 2 + x) * 2 * part, 2 * part)
        return copy(r, r, csa.at[l, j], cra.at[l, j], tp=sibling)

    def c_b(l, j, core):
        r = o_rows(l, j, (core * 2 + 1 - x) * 2 * part, 2 * part)
        return copy(r, r, csb.at[l, j], crb.at[l, j], tp=sibling)

    def sides(k):
        return ((s >= k, s - k, 1, s < sp - 1), (s + k < sp, s + k, -1, s > 0))

    below, above = s, sp - 1 - s
    paired = jnp.minimum(below, above)

    def slice_at(i):
        if i == 0:
            return s
        far = (i + 1) // 2
        near = s - far if i % 2 else s + far
        rest = jnp.where(below > above, s - (i - paired), s + (i - paired))
        return jnp.where(i <= 2 * paired, near, rest)

    at_end = jnp.logical_or(s == 0, s == sp - 1)
    inside = jnp.logical_not(at_end)

    def own(l, cond):
        for p in range(PIECES):
            for way, can in ((1, s < sp - 1), (-1, s > 0)):
                start(both(cond, can), lambda way=way, p=p: z_w(l, s, way, p))
        for way, can in ((1, s < sp - 1), (-1, s > 0)):
            start(both(cond, can), lambda way=way: z_o(l, s, way))

    def pump_w(l, k, pieces):
        for p in pieces:
            for has, j, way, more in sides(k):
                when(has, lambda: z_w(l, j, way, p).wait_recv())
                start(both(has, more), lambda l=l, j=j, way=way, p=p: z_w(l, j, way, p))
                start(has, lambda l=l, j=j, p=p: y_w(l, j, g, p))

    def pump_o(l, k):
        for has, j, way, more in sides(k):
            when(has, lambda: z_o(l, j, way).wait_recv())
            start(both(has, more), lambda l=l, j=j, way=way: z_o(l, j, way))
            start(has, lambda l=l, j=j: y_o(l, j, g))
            start(has, lambda l=l, j=j: x_a(l, j, x))
            if l == layers - 1:
                start(both(has, j == slice_at(sp - 1)), lambda: d_o(x, g))

    def pump(l, k):
        pump_w(l, k, range(PIECES))
        pump_o(l, k)

    def direct(l, i):
        return l == layers - 1 and i == sp - 1

    def x_phase(l, i):
        j = slice_at(i)
        y_o(l, j, 1 - g).wait_recv()
        if not direct(l, i):
            start(None, lambda: x_b(l, j, x))
        start(None, lambda: c_a(l, j, c))

    def c_phase(l, i):
        j = slice_at(i)
        x_a(l, j, 1 - x).wait_recv()
        if direct(l, i):
            d_o(1 - x, 1 - g).wait_recv()
        else:
            x_b(l, j, 1 - x).wait_recv()
        start(None, lambda: c_b(l, j, c))

    def c_wait(l, i):
        c_a(l, slice_at(i), 1 - c).wait_recv()
        c_b(l, slice_at(i), 1 - c).wait_recv()

    def local_weights(l):
        made = [
            pltpu.make_async_copy(src.at[l], w.at[l, s, :, pl.ds(i * ch, ch)], loc.at[l, i])
            for i, src in enumerate((gate_hbm, conv_hbm, value_hbm))
        ]
        return made + [pltpu.make_async_copy(outw_hbm.at[l], ow.at[l, s], loc.at[l, 3])]

    def wait_local(l):
        for one in local_weights(l):
            one.wait()

    tok_copy = pltpu.make_async_copy(tok_hbm, tok, loc.at[layers, 0])
    small_copies = [
        pltpu.make_async_copy(src, dst, small.at[i])
        for i, (src, dst) in enumerate(
            ((taps_hbm, taps_ref), (pre_hbm, pre_ref), (mixg_hbm, mixg_ref), (post_hbm, post_ref))
        )
    ]

    barrier = pltpu.get_barrier_semaphore()

    def greet(**device):
        pl.semaphore_signal(barrier, inc=1, device_id=device, device_id_type=MESH)

    pl.when(s > 0)(lambda: greet(sp=s - 1))
    pl.when(s < sp - 1)(lambda: greet(sp=s + 1))
    greet(grp=1 - g)
    greet(tp=sibling)
    greet(tp=across)
    greet(tp=diagonal)
    for l in range(layers):
        for one in local_weights(l):
            one.start()
        if l == 0:
            tok_copy.start()
            for one in small_copies:
                one.start()
    pl.semaphore_wait(barrier, jnp.where(at_end, 5, 6))

    wait_local(0)
    own(0, None)

    block = VPU_ROWS
    big = rows // 2
    tok_copy.wait()
    for one in small_copies:
        one.wait()

    def first_norm(i, carry):
        at = pl.ds(pl.multiple_of(i * block, block), block)
        v = tok[at, :].astype(jnp.float32)
        scale = lax.rsqrt(jnp.sum(v * v, axis=-1, keepdims=True) * (1.0 / width) + EPS)
        nrm[at, :] = (v * scale * pre_ref[0:1, :]).astype(jnp.bfloat16)
        return carry

    def term(l, i, at):
        j = slice_at(i)
        across_depth = pl.ds(pl.multiple_of(j * depth, depth), depth)
        return jnp.dot(nrm[at, across_depth], w[l, j], preferred_element_type=jnp.float32)

    def arrived(l, i):
        j = slice_at(i)
        for p in range(PIECES):
            y_w(l, j, 1 - g, p).wait_recv()

    def add_term(l, i):
        if i > 0:
            arrived(l, i)
        for piece in range(rows // big):
            at = pl.ds(piece * big, big)
            if i == 0:
                acc[at, :] = term(l, i, at)
            else:
                acc[at, :] += term(l, i, at)

    hrows = halo_tx.shape[0]

    def halo():
        return copy(halo_tx, halo_rx, hs.at[0], hr_sem.at[0], sp=s + 1)

    def tail():
        return copy(
            nrm.at[pl.ds(rows - 8, 8), :], nrm.at[pl.ds(rows, 8), :], hs.at[1], hr_sem.at[1], sp=s + 1
        )

    def tail_terms(l):
        pl.when(s > 0)(lambda: tail().wait_recv())
        at = pl.ds(rows, 8)
        total = term(l, 0, at)
        for i in range(1, sp - 1):
            total = total + term(l, i, at)
        acc[at, :] = total

    def last_term(l):
        arrived(l, sp - 1)
        for piece in reversed(range(rows // big)):
            first = piece == rows // big - 1
            extra = 8 if l > 0 and first else 0
            at = pl.ds(piece * big, big + extra)
            prod = (acc[at, :] + term(l, sp - 1, at)).astype(jnp.bfloat16)
            outer[pl.ds(piece * big, big), :] = prod[:big, :ch]
            gated = (
                prod[:, ch : 2 * ch].astype(jnp.float32) * prod[:, 2 * ch :].astype(jnp.float32)
            ).astype(jnp.bfloat16)
            wide = gated.astype(jnp.float32)
            gpad[pl.ds(8 + piece * big, big), :] = wide[:big]
            if extra:
                gpad[0:8, :] = wide[big:]
            elif first:
                halo_tx[...] = gated[big - hrows :, :]
                start(s < sp - 1, halo)

    def fill_halo():
        @pl.when(s == 0)
        def _():
            gpad[0:8, :] = jnp.zeros((8, ch), jnp.float32)

        @pl.when(s > 0)
        def _():
            halo().wait_recv()
            gpad[0:8, :] = halo_rx[...].astype(jnp.float32)[hrows - 8 :, :]

    def convolved(l, piece):
        at = pl.ds(piece * share, share)
        filtered = jnp.zeros((share, ch), jnp.float32)
        for k in range(taps):
            tap = taps_ref[k, l : l + 1, pl.ds(pl.multiple_of(t * ch, ch), ch)]
            filtered = filtered + tap * gpad[pl.ds(8 - (taps - 1) + k + piece * share, share), :]
        return (outer[at, :].astype(jnp.float32) * filtered).astype(jnp.bfloat16)

    def tp_copy(l, j, piece, kind, to):
        r = m.at[l, j, pl.ds(piece * share, share), :]
        return copy(r, r, ts.at[l, kind, piece], tr.at[l, j, piece], tp=to)

    def mix(l, read):
        parts = [read(j).astype(jnp.float32) for j in range(tp)]
        total = parts[0] * parts[0]
        for one in parts[1:]:
            total = total + one * one
        scale = lax.rsqrt(jnp.sum(total, axis=-1, keepdims=True) * (1.0 / (tp * ch)) + EPS)
        return jnp.concatenate([
            (one * scale * mixg_ref[l : l + 1, j * ch : (j + 1) * ch]).astype(jnp.bfloat16)
            for j, one in enumerate(parts)
        ], axis=1)

    def project(l, mixed, j):
        at = pl.ds(j * cols, cols) if isinstance(j, int) else pl.ds(pl.multiple_of(j * cols, cols), cols)
        br[pl.ds(0, mixed.shape[0]), at] = jnp.dot(
            mixed, ow[l, j], preferred_element_type=jnp.float32
        ).astype(jnp.bfloat16).astype(jnp.float32)

    @pl.when(s == 0)
    def _():
        nrm[pl.ds(rows, 8), :] = jnp.zeros((8, width), jnp.bfloat16)

    lax.fori_loop(0, rows // block, first_norm, 0)
    wait_local(1)
    own(1, at_end)
    add_term(0, 0)
    pump(0, 1)
    for k in range(2, sp):
        pump(0, k)
        if k == sp - 2:
            own(1, inside)
        add_term(0, k - 1)
        x_phase(0, k - 1)
        if k > 2:
            c_phase(0, k - 2)

    early = len(pending)
    quarters = [range(n * PIECES // 4, (n + 1) * PIECES // 4) for n in range(4)]
    pump_w(1, 1, quarters[0])
    l = 0
    last_term(l)
    pump_w(1, 1, quarters[1])
    for piece in reversed(range(tp)):
        if piece == 0:
            fill_halo()
        m[l, t, pl.ds(piece * share, share), :] = convolved(l, piece)
        start(None, lambda piece=piece: tp_copy(0, t, piece, 0, across))
        start(None, lambda piece=piece: tp_copy(0, t, piece, 1, sibling))
    pump_w(1, 1, quarters[2])
    x_phase(l, sp - 1)
    c_phase(l, sp - 2)
    pump_w(1, 1, quarters[3])
    for piece in reversed(range(tp)):
        tp_copy(l, across, piece, 0, across).wait_recv()
        start(None, lambda piece=piece: tp_copy(0, across, piece, 2, sibling))
        if piece == tp - 1:
            pump_o(1, 1)
    pump_w(1, 2, quarters[0])
    c_phase(l, sp - 1)
    for i in range(1, sp):
        c_wait(l, i)
    for half_index, piece in enumerate(reversed(range(rows // big))):
        for inner in reversed(range(piece * tp // 2, (piece + 1) * tp // 2)):
            tp_copy(l, sibling, inner, 1, sibling).wait_recv()
            tp_copy(l, diagonal, inner, 2, sibling).wait_recv()
        at = pl.ds(piece * big, big)
        mixed = mix(l, lambda j: m[l, j, at, :])
        for j in range(sp):
            project(l, mixed, j)
            if half_index == 0 and j == sp // 2 - 1:
                pump_w(1, 2, quarters[1])
        if half_index == 0:
            pump_w(1, 2, quarters[2])
        else:
            for k in range(3, sp):
                pump_w(1, k, quarters[0])

        def next_rows(i, carry):
            within = pl.ds(pl.multiple_of(i * block, block), block)
            first = piece * big + i * block
            whole = pl.ds(pl.multiple_of(first, block), block)
            b = br[within, :]
            scale = lax.rsqrt(jnp.sum(b * b, axis=-1, keepdims=True) * (1.0 / width) + EPS)
            v = tok[whole, :].astype(jnp.float32) + b * scale * post_ref[l : l + 1, :]

            @pl.when(first // share == t)
            def _():
                res[pl.ds(pl.multiple_of(first - t * share, block), block), :] = v

            scale = lax.rsqrt(jnp.sum(v * v, axis=-1, keepdims=True) * (1.0 / width) + EPS)
            nrm[whole, :] = (v * scale * pre_ref[l + 1 : l + 2, :]).astype(jnp.bfloat16)
            return carry

        lax.fori_loop(0, big // block, next_rows, 0)
        if half_index == 0:
            start(s < sp - 1, tail)
            pump_w(1, 2, quarters[3])
            pump_o(1, 2)
        else:
            for k in range(3, sp):
                pump_w(1, k, quarters[1])

    l = 1
    add_term(l, 0)
    add_term(l, 1)
    for k in range(3, sp):
        pump_w(1, k, quarters[2])
    x_phase(l, 1)
    for k in range(3, sp):
        add_term(l, k - 1)
        pump_w(1, k, quarters[3])
        x_phase(l, k - 1)
        c_phase(l, k - 2)
        pump_o(1, k)
    tail_terms(l)
    flush(early)
    last_term(l)
    for piece in reversed(range(tp)):
        at = pl.ds(piece * share, share)
        raw = convolved(l, piece)
        ms[at, :] = raw

        @pl.when(t == piece)
        def _():
            mlast[t] = raw

        start(t != piece, lambda at=at, piece=piece: copy(
            ms.at[at, :], mlast.at[t], a2s.at[piece], a2r.at[t], tp=piece))
    c_phase(l, sp - 2)
    x_phase(l, sp - 1)
    c_phase(l, sp - 1)
    for piece in range(tp):
        @pl.when(t != piece)
        def _():
            copy(ms.at[pl.ds(0, share), :], mlast.at[piece], a2s.at[piece], a2r.at[piece], tp=piece).wait_recv()
    mixed = mix(l, lambda j: mlast[j])
    for i in range(sp):
        if i > 0:
            c_wait(l, i)
        project(l, mixed, slice_at(i))

    def last_rows(i, carry):
        at = pl.ds(pl.multiple_of(i * block, block), block)
        b = br[at, :]
        scale = lax.rsqrt(jnp.sum(b * b, axis=-1, keepdims=True) * (1.0 / width) + EPS)
        out_ref[at, :] = (res[at, :] + b * scale * post_ref[l : l + 1, :]).astype(jnp.bfloat16)
        return carry

    lax.fori_loop(0, share // block, last_rows, 0)
    flush()


VPU_ROWS = 64
PIECES = 4
VMEM_GRANT = 63 * 1024 * 1024


def fused(sizes, tokens, gate_in, gate_conv, value_in, out_weight, conv_taps, pre_gain, mix_gain, post_gain):
    layers, grp, sp, tp, ch, rows, depth, cols = sizes
    width = sp * cols
    share = rows // tp
    bf, f32 = jnp.bfloat16, jnp.float32
    dma = pltpu.SemaphoreType.DMA
    hbm = pl.BlockSpec(memory_space=pltpu.HBM)
    vmem = pl.BlockSpec(memory_space=pltpu.VMEM)
    taps = jnp.transpose(conv_taps, (1, 0, 2))
    held = pl.pallas_call(
        functools.partial(fused_kernel, sizes),
        out_shape=pltpu.VMEM((share, width), bf),
        in_specs=[hbm] * 9,
        out_specs=vmem,
        scratch_shapes=[
            pltpu.VMEM(taps.shape, f32),
            pltpu.VMEM(pre_gain.shape, f32),
            pltpu.VMEM(mix_gain.shape, f32),
            pltpu.VMEM(post_gain.shape, f32),
            pltpu.VMEM((rows, width), bf),
            pltpu.VMEM((rows + 8, width), bf),
            pltpu.VMEM((layers, sp, depth, 3 * ch), bf),
            pltpu.VMEM((layers, sp, tp * ch, cols), bf),
            pltpu.VMEM((8 + rows, ch), f32),
            pltpu.VMEM((rows, ch), bf),
            pltpu.VMEM((rows + 8, 3 * ch), f32),
            pltpu.VMEM((16, ch), bf),
            pltpu.VMEM((16, ch), bf),
            pltpu.VMEM((max(layers - 1, 1), tp, rows, ch), bf),
            pltpu.VMEM((rows, ch), bf),
            pltpu.VMEM((tp, share, ch), bf),
            pltpu.VMEM((rows // 2, width), f32),
            pltpu.VMEM((share, width), f32),
            dma((layers + 1, 4)),
            dma((layers, 2, sp, PIECES)), dma((layers, sp, PIECES)),
            dma((layers, 2, sp)), dma((layers, sp)),
            dma((layers, sp, PIECES)), dma((layers, sp, PIECES)),
            dma((layers, sp)), dma((layers, sp)),
            dma((layers, sp)), dma((layers, sp)),
            dma((layers, sp)), dma((layers, sp)),
            dma((layers, sp)), dma((layers, sp)),
            dma((1,)), dma((1,)),
            dma((layers, sp)), dma((layers, sp)),
            dma((2,)), dma((2,)),
            dma((max(layers - 1, 1), 3, tp)), dma((max(layers - 1, 1), tp, tp)),
            dma((tp,)), dma((tp,)), dma((4,)),
        ],
        compiler_params=pltpu.CompilerParams(
            collective_id=0, has_side_effects=True, vmem_limit_bytes=VMEM_GRANT
        ),
    )(tokens, gate_in, gate_conv, value_in, out_weight, taps, pre_gain, mix_gain, post_gain)
    return held


def fits(sizes, taps):
    layers, grp, sp, tp, ch, rows, depth, cols = sizes
    width = sp * cols
    share = rows // tp
    held = rows * width * 4 + layers * sp * depth * 6 * ch + layers * tp * ch * width * 2
    held += rows * width * 2 + share * width * 8 + layers * tp * rows * ch * 2
    return (
        grp == 2 and tp == 4 and 4 <= sp <= 8 and layers == 2 and taps <= 9
        and ch % 128 == 0 and cols % 128 == 0 and rows % 512 == 0 and depth % 256 == 0
        and held < 40 * 1024 * 1024
    )


def chosen(*arrays):
    tokens, gate_in, _, _, out_weight, conv_taps = arrays[:6]
    sizes = (
        gate_in.shape[0], lax.axis_size("grp"), lax.axis_size("sp"), lax.axis_size("tp"),
        gate_in.shape[2], tokens.shape[0], gate_in.shape[1], out_weight.shape[2],
    )
    if fits(sizes, conv_taps.shape[1]):
        return fused(sizes, *arrays)
    return per_device(*arrays)


def solution(mesh):
    placed = (
        P(("grp", "sp"), None),
        P(None, "sp", "tp"),
        P(None, "sp", "tp"),
        P(None, "sp", "tp"),
        P(None, None, "sp"),
        P(),
        P(),
        P(),
        P(),
    )
    return jax.shard_map(
        chosen,
        mesh=mesh,
        in_specs=placed,
        out_specs=P(("grp", "sp", "tp"), None),
        check_vma=False,
    )
```

time: 62.3 us -> 53.7 us (0.86)
  Pallas kernels: 61.3 us -> 52.8 us
    pallas_call x1, Pallas kernels: 61.3 us -> 52.8 us  [fused(): pl.pallas_call(functools.partial(fused_kernel, sizes), out_shape=pltpu.VM...]
where the time goes in v2:
time: 53.7 us; the launch traced here: 53.6 us
  Pallas kernels  52.8 us (98%)
  local copies, waits for them, and re-layouts  0.8 us (1%)
    pallas_call x1, Pallas kernels, fused(): pl.pallas_call(functools.partial(fused_kernel, sizes), out_shape=pltpu.VM...  52.8 us

profile of v2, /device:TPU:0, one launch (start us, length us, event | category | flops | bytes accessed | tf_op | source)
XLA Modules:
  0.0 53.6 jit_solution(10121981451658759556)
XLA Ops:
  0.0 52.8 %shard_map.91 = bf16[128,2048]{1,0:T(8,128)(2,1)S(1)} custom-call(bf16[512,2048]{1,0:T(8,128)(2,1)} %tok_hbm.1, bf16[2,512,128]{2,1,0:T(8,128)(2,1)} %gate_hbm.1, bf16[2,512,128]{2,1,0:T(8,128)(2,1)} %conv_hbm.1, bf16[2,512,128]{2,1,0:T(8,128)(2,1)} %value_hbm.1, bf16[2,512,512]{2,1,0:T(8,128)(2,1)} %outw_hbm.1, f32[3,2,512]{2,1,0:T(2,128)} %bitcast.1, ...), custom_call_target="tpu_custom_call" | custom-call | tf_op jit(solution)/shard_map/pallas_call | solution.py:540
  52.8 0.8 %copy.11 = bf16[128,2048]{1,0:T(8,128)(2,1)} copy(bf16[128,2048]{1,0:T(8,128)(2,1)S(1)} %shard_map.91) | data formatting | bytes 1048576

commit v3 on v2

--- a/solution.py
+++ b/solution.py
@@ -79,7 +79,8 @@
     tok_hbm, gate_hbm, conv_hbm, value_hbm, outw_hbm, taps_hbm, pre_hbm, mixg_hbm, post_hbm,
     out_ref, taps_ref, pre_ref, mixg_ref, post_ref,
     tok, nrm, w, ow, gpad, outer, acc, halo_tx, halo_rx, m, ms, mlast, br, res,
-    loc, zsw, zrw, zso, zro, ysw, yrw, yso, yro, xsa, xra, xsb, xrb, csa, cra, dso, dro, csb, crb, hs, hr_sem, ts, tr, a2s, a2r, small,
+    lw, lo, lt, small, zsw, zrw, zso, zro, ysw, yrw, yso, yro, xs, xr, cs, cr,
+    hs, hr_sem, ts, tra, trs, trd, a2s, a2r,
 ):
     layers, grp, sp, tp, ch, rows, depth, cols = sizes
     width = sp * cols
@@ -95,8 +96,6 @@
     share = rows // tp
     half = depth // 2
     part = (tp * ch) // (2 * tp)
-    pending = []
-
     def when(cond, body):
         if cond is None:
             body()
@@ -114,13 +113,6 @@
 
     def start(cond, make):
         when(cond, lambda: make().start())
-        pending.append((cond, make))
-
-    def flush(count=None):
-        count = len(pending) if count is None else count
-        for cond, make in pending[:count]:
-            when(cond, lambda: make().wait_send())
-        del pending[:count]
 
     piece_rows = half // PIECES
 
@@ -129,47 +121,60 @@
         return w.at[l, j, pl.ds(first, piece_rows), :]
 
     def o_rows(l, j, first, count):
-        return ow.at[l, j, pl.ds(pl.multiple_of(first, part), count), :]
+        return ow.at[l, j, pl.ds(pl.multiple_of(first * part, part), count * part), :]
 
     def o_part(side, group):
-        return ((c * 2 + side) * 2 + group) * part
+        return (c * 2 + group) * 2 + side
+
+    def spot(j, at):
+        return lax.rem(j - at - 1 + 2 * sp, sp)
 
     def z_w(l, j, way, p):
         r = w_half(l, j, g, p)
-        return copy(r, r, zsw.at[l, (way + 1) // 2, j, p], zrw.at[l, j, p], sp=s + way)
-
-    def z_o(l, j, way):
-        r = o_rows(l, j, o_part(x, g), part)
-        return copy(r, r, zso.at[l, (way + 1) // 2, j], zro.at[l, j], sp=s + way)
-
-    def y_w(l, j, h, p):
-        r = w_half(l, j, h, p)
-        return copy(r, r, ysw.at[l, j, p], yrw.at[l, j, p], grp=1 - g)
-
-    def y_o(l, j, group):
-        r = o_rows(l, j, o_part(x, group), part)
-        return copy(r, r, yso.at[l, j], yro.at[l, j], grp=1 - g)
-
-    def x_a(l, j, side):
-        r = o_rows(l, j, o_part(side, g), part)
-        return copy(r, r, xsa.at[l, j], xra.at[l, j], tp=across)
-
-    def x_b(l, j, side):
-        r = o_rows(l, j, o_part(side, 1 - g), part)
-        return copy(r, r, xsb.at[l, j], xrb.at[l, j], tp=across)
-
-    def d_o(side, group):
-        l, j = layers - 1, slice_at(sp - 1)
-        r = o_rows(l, j, o_part(side, group), part)
-        return copy(r, r, dso.at[0], dro.at[0], tp=across, grp=1 - g)
-
-    def c_a(l, j, core):
-        r = o_rows(l, j, (core * 2 + x) * 2 * part, 2 * part)
-        return copy(r, r, csa.at[l, j], cra.at[l, j], tp=sibling)
-
-    def c_b(l, j, core):
-        r = o_rows(l, j, (core * 2 + 1 - x) * 2 * part, 2 * part)
-        return copy(r, r, csb.at[l, j], crb.at[l, j], tp=sibling)
+        return copy(r, r, zsw.at[(way + 1) // 2], zrw.at[l, spot(j, s + way), p], sp=s + way)
+
+    def z_w_in(l, j, way, p):
+        r = w_half(l, j, g, p)
+        return copy(r, r, zsw.at[0], zrw.at[l, spot(j, s), p], sp=s + way)
+
+    def o_first(count):
+        return {1: o_part(x, g), 2: o_part(0, g), 4: c * 4}[count]
+
+    def z_o(l, j, way, count):
+        r = o_rows(l, j, o_first(count), count)
+        return copy(r, r, zso.at[l, (way + 1) // 2], zro.at[l, spot(j, s + way)], sp=s + way)
+
+    def z_o_in(l, j, way, count):
+        r = o_rows(l, j, o_first(count), count)
+        return copy(r, r, zso.at[l, 0], zro.at[l, spot(j, s)], sp=s + way)
+
+    def y_w(l, j, p):
+        r = w_half(l, j, g, p)
+        return copy(r, r, ysw.at[0], yrw.at[l, spot(j, s)], grp=1 - g)
+
+    def y_w_in(l, j):
+        r = w.at[l, j, pl.ds(pl.multiple_of((1 - g) * half, half), half), :]
+        return copy(r, r, ysw.at[0], yrw.at[l, spot(j, s)], grp=1 - g)
+
+    def y_o(l, j, group, count):
+        r = o_rows(l, j, o_part(x if count == 1 else 0, group), count)
+        return copy(r, r, yso.at[l], yro.at[l, spot(j, s)], grp=1 - g)
+
+    def x_o(l, j, group):
+        r = o_rows(l, j, o_part(x, group), 1)
+        return copy(r, r, xs.at[l], xr.at[l, spot(j, s)], tp=across)
+
+    def x_o_in(l, j):
+        r = o_rows(l, j, c * 4, 2)
+        return copy(r, r, xs.at[l], xr.at[l, spot(j, s)], tp=across)
+
+    def c_o(l, j, core):
+        r = o_rows(l, j, core * 4, 4)
+        return copy(r, r, cs.at[0], cr.at[spot(j, s) + 1 if l else 0], tp=sibling)
+
+    def c_all(l):
+        r = ow.at[l, pl.ds(0, sp - 1), pl.ds(0, 4 * part), :]
+        return copy(r, r, cs.at[0], cr.at[0], tp=sibling)
 
     def sides(k):
         return ((s >= k, s - k, 1, s < sp - 1), (s + k < sp, s + k, -1, s > 0))
@@ -191,65 +196,145 @@
     def own(l, cond):
         for p in range(PIECES):
             for way, can in ((1, s < sp - 1), (-1, s > 0)):
-                start(both(cond, can), lambda way=way, p=p: z_w(l, s, way, p))
+                start(both(cond, can), lambda: z_w(l, s, way, p))
         for way, can in ((1, s < sp - 1), (-1, s > 0)):
-            start(both(cond, can), lambda way=way: z_o(l, s, way))
+            if l < layers - 1:
+                start(both(cond, can), lambda: z_o(l, s, way, 1))
+            else:
+                start(both(cond, jnp.logical_and(can, at_end)), lambda: z_o(l, s, way, 4))
+                start(both(cond, jnp.logical_and(can, inside)), lambda: z_o(l, s, way, 1))
 
     def pump_w(l, k, pieces):
         for p in pieces:
             for has, j, way, more in sides(k):
-                when(has, lambda: z_w(l, j, way, p).wait_recv())
-                start(both(has, more), lambda l=l, j=j, way=way, p=p: z_w(l, j, way, p))
-                start(has, lambda l=l, j=j, p=p: y_w(l, j, g, p))
-
-    def pump_o(l, k):
+                @pl.when(has)
+                def _():
+                    z_w_in(l, j, way, p).wait_recv()
+                    start(more, lambda: z_w(l, j, way, p))
+                    y_w(l, j, p).start()
+
+    def pump_o(l, k, cond=None):
         for has, j, way, more in sides(k):
-            when(has, lambda: z_o(l, j, way).wait_recv())
-            start(both(has, more), lambda l=l, j=j, way=way: z_o(l, j, way))
-            start(has, lambda l=l, j=j: y_o(l, j, g))
-            start(has, lambda l=l, j=j: x_a(l, j, x))
+            first = (s == k) if way == 1 else (s == sp - 1 - k)
+            single = has if l < layers - 1 else jnp.logical_and(has, jnp.logical_not(first))
+
+            @pl.when(both(cond, single))
+            def _():
+                z_o_in(l, j, way, 1).wait_recv()
+                start(more, lambda: z_o(l, j, way, 1))
+                y_o(l, j, g, 1).start()
+                x_o(l, j, g).start()
+
             if l == layers - 1:
-                start(both(has, j == slice_at(sp - 1)), lambda: d_o(x, g))
+                @pl.when(both(cond, jnp.logical_and(has, first)))
+                def _():
+                    z_o_in(l, j, way, 4 if k == 1 else 2).wait_recv()
+                    start(more, lambda: z_o(l, j, way, 2))
+                    if k == 1:
+                        c_o(l, j, c).start()
+                    else:
+                        y_o(l, j, g, 2).start()
 
     def pump(l, k):
         pump_w(l, k, range(PIECES))
         pump_o(l, k)
 
-    def direct(l, i):
-        return l == layers - 1 and i == sp - 1
+    def kind(l, j):
+        if l < layers - 1:
+            return None, None
+        first = jnp.logical_or(j == 0, j == sp - 1)
+        near = jnp.logical_or(j == s - 1, j == s + 1)
+        return jnp.logical_not(first), jnp.logical_and(first, jnp.logical_not(near))
 
     def x_phase(l, i):
         j = slice_at(i)
-        y_o(l, j, 1 - g).wait_recv()
-        if not direct(l, i):
-            start(None, lambda: x_b(l, j, x))
-        start(None, lambda: c_a(l, j, c))
+        single, doubled = kind(l, j)
+
+        def relay():
+            y_o(l, j, 1 - g, 1).wait_recv()
+            x_o(l, j, 1 - g).start()
+
+        def finish():
+            y_o(l, j, 1 - g, 2).wait_recv()
+            c_o(l, j, c).start()
+
+        when(single, relay)
+        if doubled is not None:
+            when(doubled, finish)
 
     def c_phase(l, i):
         j = slice_at(i)
-        x_a(l, j, 1 - x).wait_recv()
-        if direct(l, i):
-            d_o(1 - x, 1 - g).wait_recv()
-        else:
-            x_b(l, j, 1 - x).wait_recv()
-        start(None, lambda: c_b(l, j, c))
+        single, _ = kind(l, j)
+
+        def body():
+            x_o_in(l, j).wait_recv()
+            c_o(l, j, c).start()
+
+        when(single, body)
 
     def c_wait(l, i):
-        c_a(l, slice_at(i), 1 - c).wait_recv()
-        c_b(l, slice_at(i), 1 - c).wait_recv()
+        c_o(l, slice_at(i), 1 - c).wait_recv()
+
+    def parts_sent(l, at):
+        last = l == layers - 1
+        ends = (0, sp - 1)
+        others = [j for j in range(sp) if j != at]
+
+        def on_z(j):
+            if not last:
+                return 1
+            return (4 if j in ends else 1) if j == at else (2 if j in ends else 1)
+
+        up = sum(on_z(j) for j in range(at + 1)) if at < sp - 1 else 0
+        down = sum(on_z(j) for j in range(at, sp)) if at > 0 else 0
+        on_y = sum(1 if not last or j not in ends else 0 if abs(j - at) == 1 else 2 for j in others)
+        on_x = sum(2 if not last or j not in ends else 0 for j in others)
+        return up, down, on_y, on_x
+
+    def drain():
+        def sent(ref, sem, **device):
+            copy(ref, ref, sem, a2r.at[0], **device).wait_send()
+
+        def parts(l, count):
+            return ow.at[l, 0, pl.ds(0, count * part), :]
+
+        for at in range(sp):
+            @pl.when(s == at)
+            def _():
+                for way, count in ((1, at + 1), (-1, sp - at)):
+                    if 0 <= at + way < sp:
+                        sent(w.at[:, pl.ds(0, count), pl.ds(0, half), :], zsw.at[(way + 1) // 2], sp=s + way)
+                for l in range(layers):
+                    up, down, on_y, on_x = parts_sent(l, at)
+                    if up:
+                        sent(parts(l, up), zso.at[l, 1], sp=s + 1)
+                    if down:
+                        sent(parts(l, down), zso.at[l, 0], sp=s - 1)
+                    sent(parts(l, on_y), yso.at[l], grp=1 - g)
+                    if on_x:
+                        sent(parts(l, on_x), xs.at[l], tp=across)
+        sent(w.at[:, pl.ds(0, sp - 1), pl.ds(0, half), :], ysw.at[0], grp=1 - g)
+        sent(ow.at[:, pl.ds(0, sp - 1), pl.ds(0, 4 * part), :], cs.at[0], tp=sibling)
+        sent(m.at[0, pl.ds(0, 3)], ts.at[0], tp=sibling)
+        sent(mlast.at[pl.ds(0, tp - 1)], a2s.at[0], tp=sibling)
+
+        @pl.when(s < sp - 1)
+        def _():
+            halo().wait_send()
+            tail().wait_send()
 
     def local_weights(l):
         made = [
-            pltpu.make_async_copy(src.at[l], w.at[l, s, :, pl.ds(i * ch, ch)], loc.at[l, i])
+            pltpu.make_async_copy(src.at[l], w.at[l, s, :, pl.ds(i * ch, ch)], lw.at[l])
             for i, src in enumerate((gate_hbm, conv_hbm, value_hbm))
         ]
-        return made + [pltpu.make_async_copy(outw_hbm.at[l], ow.at[l, s], loc.at[l, 3])]
+        return made + [pltpu.make_async_copy(outw_hbm.at[l], ow.at[l, s], lo.at[l])]
 
     def wait_local(l):
-        for one in local_weights(l):
-            one.wait()
-
-    tok_copy = pltpu.make_async_copy(tok_hbm, tok, loc.at[layers, 0])
+        pltpu.make_async_copy(w.at[l, s], w.at[l, s], lw.at[l]).wait()
+        pltpu.make_async_copy(outw_hbm.at[l], ow.at[l, s], lo.at[l]).wait()
+
+    tok_copy = pltpu.make_async_copy(tok_hbm, tok, lt.at[0])
     small_copies = [
         pltpu.make_async_copy(src, dst, small.at[i])
         for i, (src, dst) in enumerate(
@@ -299,9 +384,7 @@
         return jnp.dot(nrm[at, across_depth], w[l, j], preferred_element_type=jnp.float32)
 
     def arrived(l, i):
-        j = slice_at(i)
-        for p in range(PIECES):
-            y_w(l, j, 1 - g, p).wait_recv()
+        y_w_in(l, slice_at(i)).wait_recv()
 
     def add_term(l, i):
         if i > 0:
@@ -368,9 +451,13 @@
             filtered = filtered + tap * gpad[pl.ds(8 - (taps - 1) + k + piece * share, share), :]
         return (outer[at, :].astype(jnp.float32) * filtered).astype(jnp.bfloat16)
 
-    def tp_copy(l, j, piece, kind, to):
-        r = m.at[l, j, pl.ds(piece * share, share), :]
-        return copy(r, r, ts.at[l, kind, piece], tr.at[l, j, piece], tp=to)
+    def tp_copy(j, piece, recv, to):
+        r = m.at[0, j, pl.ds(piece * share, share), :]
+        return copy(r, r, ts.at[0], recv, tp=to)
+
+    def tp_half(j, piece, recv):
+        r = m.at[0, j, pl.ds(piece * big, big), :]
+        return copy(r, r, ts.at[0], recv.at[piece], tp=sibling)
 
     def mix(l, read):
         parts = [read(j).astype(jnp.float32) for j in range(tp)]
@@ -407,7 +494,6 @@
         if k > 2:
             c_phase(0, k - 2)
 
-    early = len(pending)
     quarters = [range(n * PIECES // 4, (n + 1) * PIECES // 4) for n in range(4)]
     pump_w(1, 1, quarters[0])
     l = 0
@@ -417,25 +503,23 @@
         if piece == 0:
             fill_halo()
         m[l, t, pl.ds(piece * share, share), :] = convolved(l, piece)
-        start(None, lambda piece=piece: tp_copy(0, t, piece, 0, across))
-        start(None, lambda piece=piece: tp_copy(0, t, piece, 1, sibling))
+        tp_copy(t, piece, tra.at[piece], across).start()
+        tp_copy(t, piece, trs.at[piece * share // big], sibling).start()
     pump_w(1, 1, quarters[2])
     x_phase(l, sp - 1)
     c_phase(l, sp - 2)
     pump_w(1, 1, quarters[3])
     for piece in reversed(range(tp)):
-        tp_copy(l, across, piece, 0, across).wait_recv()
-        start(None, lambda piece=piece: tp_copy(0, across, piece, 2, sibling))
+        tp_copy(across, piece, tra.at[piece], across).wait_recv()
+        tp_copy(across, piece, trd.at[piece * share // big], sibling).start()
         if piece == tp - 1:
             pump_o(1, 1)
     pump_w(1, 2, quarters[0])
     c_phase(l, sp - 1)
-    for i in range(1, sp):
-        c_wait(l, i)
+    c_all(l).wait_recv()
     for half_index, piece in enumerate(reversed(range(rows // big))):
-        for inner in reversed(range(piece * tp // 2, (piece + 1) * tp // 2)):
-            tp_copy(l, sibling, inner, 1, sibling).wait_recv()
-            tp_copy(l, diagonal, inner, 2, sibling).wait_recv()
+        tp_half(sibling, piece, trs).wait_recv()
+        tp_half(diagonal, piece, trd).wait_recv()
         at = pl.ds(piece * big, big)
         mixed = mix(l, lambda j: m[l, j, at, :])
         for j in range(sp):
@@ -486,7 +570,6 @@
         c_phase(l, k - 2)
         pump_o(1, k)
     tail_terms(l)
-    flush(early)
     last_term(l)
     for piece in reversed(range(tp)):
         at = pl.ds(piece * share, share)
@@ -497,15 +580,12 @@
         def _():
             mlast[t] = raw
 
-        start(t != piece, lambda at=at, piece=piece: copy(
-            ms.at[at, :], mlast.at[t], a2s.at[piece], a2r.at[t], tp=piece))
+        start(t != piece, lambda: copy(ms.at[at, :], mlast.at[t], a2s.at[0], a2r.at[0], tp=piece))
     c_phase(l, sp - 2)
     x_phase(l, sp - 1)
     c_phase(l, sp - 1)
-    for piece in range(tp):
-        @pl.when(t != piece)
-        def _():
-            copy(ms.at[pl.ds(0, share), :], mlast.at[piece], a2s.at[piece], a2r.at[piece], tp=piece).wait_recv()
+    others = mlast.at[pl.ds(0, tp - 1)]
+    copy(others, others, a2s.at[0], a2r.at[0], tp=sibling).wait_recv()
     mixed = mix(l, lambda j: mlast[j])
     for i in range(sp):
         if i > 0:
@@ -520,7 +600,7 @@
         return carry
 
     lax.fori_loop(0, share // block, last_rows, 0)
-    flush()
+    drain()
 
 
 VPU_ROWS = 64
@@ -561,19 +641,16 @@
             pltpu.VMEM((tp, share, ch), bf),
             pltpu.VMEM((rows // 2, width), f32),
             pltpu.VMEM((share, width), f32),
-            dma((layers + 1, 4)),
-            dma((layers, 2, sp, PIECES)), dma((layers, sp, PIECES)),
-            dma((layers, 2, sp)), dma((layers, sp)),
-            dma((layers, sp, PIECES)), dma((layers, sp, PIECES)),
-            dma((layers, sp)), dma((layers, sp)),
-            dma((layers, sp)), dma((layers, sp)),
-            dma((layers, sp)), dma((layers, sp)),
-            dma((layers, sp)), dma((layers, sp)),
+            dma((layers,)), dma((layers,)), dma((1,)), dma((4,)),
+            dma((2,)), dma((layers, sp - 1, PIECES)),
+            dma((layers, 2)), dma((layers, sp - 1)),
+            dma((1,)), dma((layers, sp - 1)),
+            dma((layers,)), dma((layers, sp - 1)),
+            dma((layers,)), dma((layers, sp - 1)),
+            dma((1,)), dma((sp,)),
+            dma((2,)), dma((2,)),
+            dma((1,)), dma((tp,)), dma((2,)), dma((2,)),
             dma((1,)), dma((1,)),
-            dma((layers, sp)), dma((layers, sp)),
-            dma((2,)), dma((2,)),
-            dma((max(layers - 1, 1), 3, tp)), dma((max(layers - 1, 1), tp, tp)),
-            dma((tp,)), dma((tp,)), dma((4,)),
         ],
         compiler_params=pltpu.CompilerParams(
             collective_id=0, has_side_effects=True, vmem_limit_bytes=VMEM_GRANT
@@ -589,7 +666,7 @@
     held = rows * width * 4 + layers * sp * depth * 6 * ch + layers * tp * ch * width * 2
     held += rows * width * 2 + share * width * 8 + layers * tp * rows * ch * 2
     return (
-        grp == 2 and tp == 4 and 4 <= sp <= 8 and layers == 2 and taps <= 9
+        grp == 2 and tp == 4 and sp == 4 and layers == 2 and taps <= 9
         and ch % 128 == 0 and cols % 128 == 0 and rows % 512 == 0 and depth % 256 == 0
         and held < 40 * 1024 * 1024
     )

time: 53.7 us -> 51.3 us (0.955)
  Pallas kernels: 52.8 us -> 50.4 us
    pallas_call x1, Pallas kernels: 52.8 us -> 50.4 us  [fused(): pl.pallas_call(functools.partial(fused_kernel, sizes), out_shape=pltpu.VM...]
where the time goes in v3:
time: 51.3 us; the launch traced here: 51.2 us
  Pallas kernels  50.4 us (98%)
  local copies, waits for them, and re-layouts  0.8 us (2%)
    pallas_call x1, Pallas kernels, fused(): pl.pallas_call(functools.partial(fused_kernel, sizes), out_shape=pltpu.VM...  50.4 us

profile of v3, /device:TPU:0, one launch (start us, length us, event | category | flops | bytes accessed | tf_op | source)
XLA Modules:
  0.0 51.2 jit_solution(2391424573552573072)
XLA Ops:
  0.0 50.4 %shard_map.91 = bf16[128,2048]{1,0:T(8,128)(2,1)S(1)} custom-call(bf16[512,2048]{1,0:T(8,128)(2,1)} %tok_hbm.1, bf16[2,512,128]{2,1,0:T(8,128)(2,1)} %gate_hbm.1, bf16[2,512,128]{2,1,0:T(8,128)(2,1)} %conv_hbm.1, bf16[2,512,128]{2,1,0:T(8,128)(2,1)} %value_hbm.1, bf16[2,512,512]{2,1,0:T(8,128)(2,1)} %outw_hbm.1, f32[3,2,512]{2,1,0:T(2,128)} %bitcast.1, ...), custom_call_target="tpu_custom_call" | custom-call | tf_op jit(solution)/shard_map/pallas_call | solution.py:620
  50.4 0.8 %copy.11 = bf16[128,2048]{1,0:T(8,128)(2,1)} copy(bf16[128,2048]{1,0:T(8,128)(2,1)S(1)} %shard_map.91) | data formatting | bytes 1048576

commit v4 on v3

--- a/solution.py
+++ b/solution.py
@@ -78,7 +78,7 @@
     sizes,
     tok_hbm, gate_hbm, conv_hbm, value_hbm, outw_hbm, taps_hbm, pre_hbm, mixg_hbm, post_hbm,
     out_ref, taps_ref, pre_ref, mixg_ref, post_ref,
-    tok, nrm, w, ow, gpad, outer, acc, halo_tx, halo_rx, m, ms, mlast, br, res,
+    tok, nrm, w, ow, gpad, outer, acc, tail_tx, tail_rx, m, ms, mlast, br, res,
     lw, lo, lt, small, zsw, zrw, zso, zro, ysw, yrw, yso, yro, xs, xr, cs, cr,
     hs, hr_sem, ts, tra, trs, trd, a2s, a2r,
 ):
@@ -137,16 +137,18 @@
         r = w_half(l, j, g, p)
         return copy(r, r, zsw.at[0], zrw.at[l, spot(j, s), p], sp=s + way)
 
-    def o_first(count):
-        return {1: o_part(x, g), 2: o_part(0, g), 4: c * 4}[count]
-
-    def z_o(l, j, way, count):
-        r = o_rows(l, j, o_first(count), count)
-        return copy(r, r, zso.at[l, (way + 1) // 2], zro.at[l, spot(j, s + way)], sp=s + way)
-
-    def z_o_in(l, j, way, count):
-        r = o_rows(l, j, o_first(count), count)
-        return copy(r, r, zso.at[l, 0], zro.at[l, spot(j, s)], sp=s + way)
+    def o_piece(l, j, count, q):
+        first = {1: o_part(x, g), 2: o_part(0, g), 4: c * 4}[count]
+        size = count * part // 2
+        return ow.at[l, j, pl.ds(pl.multiple_of(first * part + q * size, size), size), :]
+
+    def z_o(l, j, way, count, q):
+        r = o_piece(l, j, count, q)
+        return copy(r, r, zso.at[l, (way + 1) // 2], zro.at[l, spot(j, s + way), q], sp=s + way)
+
+    def z_o_in(l, j, way, count, q):
+        r = o_piece(l, j, count, q)
+        return copy(r, r, zso.at[l, 0], zro.at[l, spot(j, s), q], sp=s + way)
 
     def y_w(l, j, p):
         r = w_half(l, j, g, p)
@@ -156,8 +158,12 @@
         r = w.at[l, j, pl.ds(pl.multiple_of((1 - g) * half, half), half), :]
         return copy(r, r, ysw.at[0], yrw.at[l, spot(j, s)], grp=1 - g)
 
-    def y_o(l, j, group, count):
-        r = o_rows(l, j, o_part(x if count == 1 else 0, group), count)
+    def y_o(l, j, count, q):
+        r = o_piece(l, j, count, q)
+        return copy(r, r, yso.at[l], yro.at[l, spot(j, s)], grp=1 - g)
+
+    def y_o_in(l, j, count):
+        r = o_rows(l, j, o_part(x if count == 1 else 0, 1 - g), count)
         return copy(r, r, yso.at[l], yro.at[l, spot(j, s)], grp=1 - g)
 
     def x_o(l, j, group):
@@ -197,12 +203,13 @@
         for p in range(PIECES):
             for way, can in ((1, s < sp - 1), (-1, s > 0)):
                 start(both(cond, can), lambda: z_w(l, s, way, p))
-        for way, can in ((1, s < sp - 1), (-1, s > 0)):
-            if l < layers - 1:
-                start(both(cond, can), lambda: z_o(l, s, way, 1))
-            else:
-                start(both(cond, jnp.logical_and(can, at_end)), lambda: z_o(l, s, way, 4))
-                start(both(cond, jnp.logical_and(can, inside)), lambda: z_o(l, s, way, 1))
+        for q in range(2):
+            for way, can in ((1, s < sp - 1), (-1, s > 0)):
+                if l < layers - 1:
+                    start(both(cond, can), lambda: z_o(l, s, way, 1, q))
+                else:
+                    start(both(cond, jnp.logical_and(can, at_end)), lambda: z_o(l, s, way, 4, q))
+                    start(both(cond, jnp.logical_and(can, inside)), lambda: z_o(l, s, way, 1, q))
 
     def pump_w(l, k, pieces):
         for p in pieces:
@@ -213,31 +220,42 @@
                     start(more, lambda: z_w(l, j, way, p))
                     y_w(l, j, p).start()
 
-    def pump_o(l, k, cond=None):
+    def pump_o(l, k, q):
         for has, j, way, more in sides(k):
             first = (s == k) if way == 1 else (s == sp - 1 - k)
             single = has if l < layers - 1 else jnp.logical_and(has, jnp.logical_not(first))
 
-            @pl.when(both(cond, single))
+            @pl.when(single)
             def _():
-                z_o_in(l, j, way, 1).wait_recv()
-                start(more, lambda: z_o(l, j, way, 1))
-                y_o(l, j, g, 1).start()
-                x_o(l, j, g).start()
+                z_o_in(l, j, way, 1, q).wait_recv()
+                start(more, lambda: z_o(l, j, way, 1, q))
+                y_o(l, j, 1, q).start()
+                if q == 1:
+                    x_o(l, j, g).start()
 
             if l == layers - 1:
-                @pl.when(both(cond, jnp.logical_and(has, first)))
+                @pl.when(jnp.logical_and(has, first))
                 def _():
-                    z_o_in(l, j, way, 4 if k == 1 else 2).wait_recv()
-                    start(more, lambda: z_o(l, j, way, 2))
-                    if k == 1:
+                    z_o_in(l, j, way, 4 if k == 1 else 2, q).wait_recv()
+                    if k > 1:
+                        start(more, lambda: z_o(l, j, way, 2, q))
+                        y_o(l, j, 2, q).start()
+                    elif q == 1:
+                        for each in range(2):
+                            start(more, lambda: z_o(l, j, way, 2, each))
                         c_o(l, j, c).start()
-                    else:
-                        y_o(l, j, g, 2).start()
 
     def pump(l, k):
         pump_w(l, k, range(PIECES))
-        pump_o(l, k)
+        pump_o(l, k, 0)
+        pump_o(l, k, 1)
+
+    def pumps(l, k):
+        if k >= sp:
+            return []
+        return [lambda p=p: pump_w(l, k, [p]) for p in range(PIECES)] + [
+            lambda q=q: pump_o(l, k, q) for q in range(2)
+        ]
 
     def kind(l, j):
         if l < layers - 1:
@@ -251,11 +269,11 @@
         single, doubled = kind(l, j)
 
         def relay():
-            y_o(l, j, 1 - g, 1).wait_recv()
+            y_o_in(l, j, 1).wait_recv()
             x_o(l, j, 1 - g).start()
 
         def finish():
-            y_o(l, j, 1 - g, 2).wait_recv()
+            y_o_in(l, j, 2).wait_recv()
             c_o(l, j, c).start()
 
         when(single, relay)
@@ -291,10 +309,10 @@
         on_x = sum(2 if not last or j not in ends else 0 for j in others)
         return up, down, on_y, on_x
 
+    def sent(ref, sem, **device):
+        copy(ref, ref, sem, a2r.at[0], **device).wait_send()
+
     def drain():
-        def sent(ref, sem, **device):
-            copy(ref, ref, sem, a2r.at[0], **device).wait_send()
-
         def parts(l, count):
             return ow.at[l, 0, pl.ds(0, count * part), :]
 
@@ -314,14 +332,12 @@
                     if on_x:
                         sent(parts(l, on_x), xs.at[l], tp=across)
         sent(w.at[:, pl.ds(0, sp - 1), pl.ds(0, half), :], ysw.at[0], grp=1 - g)
-        sent(ow.at[:, pl.ds(0, sp - 1), pl.ds(0, 4 * part), :], cs.at[0], tp=sibling)
         sent(m.at[0, pl.ds(0, 3)], ts.at[0], tp=sibling)
-        sent(mlast.at[pl.ds(0, tp - 1)], a2s.at[0], tp=sibling)
 
         @pl.when(s < sp - 1)
         def _():
-            halo().wait_send()
-            tail().wait_send()
+            for l in range(layers):
+                tail(l).wait_send()
 
     def local_weights(l):
         made = [
@@ -396,29 +412,37 @@
             else:
                 acc[at, :] += term(l, i, at)
 
-    hrows = halo_tx.shape[0]
-
-    def halo():
-        return copy(halo_tx, halo_rx, hs.at[0], hr_sem.at[0], sp=s + 1)
-
-    def tail():
-        return copy(
-            nrm.at[pl.ds(rows - 8, 8), :], nrm.at[pl.ds(rows, 8), :], hs.at[1], hr_sem.at[1], sp=s + 1
-        )
+    kept = tail_tx.shape[1]
+
+    def tail(l):
+        return copy(tail_tx.at[l], tail_rx.at[l], hs.at[l], hr_sem.at[l], sp=s + 1)
+
+    def send_tail(l):
+        ending = nrm[pl.ds(rows - 8, 8), :].astype(jnp.float32)
+        tail_tx[l] = ending[8 - kept :, :].astype(jnp.bfloat16)
+        start(s < sp - 1, lambda: tail(l))
 
     def tail_terms(l):
-        pl.when(s > 0)(lambda: tail().wait_recv())
+        @pl.when(s > 0)
+        def _():
+            tail(l).wait_recv()
+            before = jnp.zeros((8 - kept, width), jnp.float32)
+            ending = jnp.concatenate([before, tail_rx[l].astype(jnp.float32)], axis=0)
+            nrm[pl.ds(rows, 8), :] = ending.astype(jnp.bfloat16)
+
         at = pl.ds(rows, 8)
         total = term(l, 0, at)
         for i in range(1, sp - 1):
             total = total + term(l, i, at)
         acc[at, :] = total
 
-    def last_term(l):
+    def last_term(l, waiting=()):
         arrived(l, sp - 1)
+        for one in waiting:
+            one()
         for piece in reversed(range(rows // big)):
             first = piece == rows // big - 1
-            extra = 8 if l > 0 and first else 0
+            extra = 8 if first else 0
             at = pl.ds(piece * big, big + extra)
             prod = (acc[at, :] + term(l, sp - 1, at)).astype(jnp.bfloat16)
             outer[pl.ds(piece * big, big), :] = prod[:big, :ch]
@@ -429,19 +453,6 @@
             gpad[pl.ds(8 + piece * big, big), :] = wide[:big]
             if extra:
                 gpad[0:8, :] = wide[big:]
-            elif first:
-                halo_tx[...] = gated[big - hrows :, :]
-                start(s < sp - 1, halo)
-
-    def fill_halo():
-        @pl.when(s == 0)
-        def _():
-            gpad[0:8, :] = jnp.zeros((8, ch), jnp.float32)
-
-        @pl.when(s > 0)
-        def _():
-            halo().wait_recv()
-            gpad[0:8, :] = halo_rx[...].astype(jnp.float32)[hrows - 8 :, :]
 
     def convolved(l, piece):
         at = pl.ds(piece * share, share)
@@ -481,6 +492,7 @@
         nrm[pl.ds(rows, 8), :] = jnp.zeros((8, width), jnp.bfloat16)
 
     lax.fori_loop(0, rows // block, first_norm, 0)
+    send_tail(0)
     wait_local(1)
     own(1, at_end)
     add_term(0, 0)
@@ -494,43 +506,55 @@
         if k > 2:
             c_phase(0, k - 2)
 
-    quarters = [range(n * PIECES // 4, (n + 1) * PIECES // 4) for n in range(4)]
-    pump_w(1, 1, quarters[0])
+    near = pumps(1, 1)
+    for one in near[:3]:
+        one()
     l = 0
-    last_term(l)
-    pump_w(1, 1, quarters[1])
-    for piece in reversed(range(tp)):
-        if piece == 0:
-            fill_halo()
+    tail_terms(l)
+    last_term(l, near[3:4])
+
+    def send_mixed(piece):
         m[l, t, pl.ds(piece * share, share), :] = convolved(l, piece)
         tp_copy(t, piece, tra.at[piece], across).start()
         tp_copy(t, piece, trs.at[piece * share // big], sibling).start()
-    pump_w(1, 1, quarters[2])
+
+    for piece in reversed(range(tp)):
+        send_mixed(piece)
+    for one in near[4:6]:
+        one()
     x_phase(l, sp - 1)
+    for one in near[6:8]:
+        one()
     c_phase(l, sp - 2)
-    pump_w(1, 1, quarters[3])
+    mid = pumps(1, 2)
+    far = [one for k in range(3, sp) for one in pumps(1, k)]
+    between = {3: near[8:10], 2: [], 1: mid[0:2], 0: mid[2:4]}
     for piece in reversed(range(tp)):
         tp_copy(across, piece, tra.at[piece], across).wait_recv()
         tp_copy(across, piece, trd.at[piece * share // big], sibling).start()
-        if piece == tp - 1:
-            pump_o(1, 1)
-    pump_w(1, 2, quarters[0])
+        for one in between[piece]:
+            one()
     c_phase(l, sp - 1)
     c_all(l).wait_recv()
+    steps = iter([
+        mid[4:5], mid[5:6], mid[6:8], mid[8:9], mid[9:10],
+        [], far[0:2], far[2:3], far[3:4], far[4:6],
+    ])
+
+    def advance():
+        for one in next(steps):
+            one()
+
     for half_index, piece in enumerate(reversed(range(rows // big))):
         tp_half(sibling, piece, trs).wait_recv()
         tp_half(diagonal, piece, trd).wait_recv()
+        advance()
         at = pl.ds(piece * big, big)
         mixed = mix(l, lambda j: m[l, j, at, :])
         for j in range(sp):
             project(l, mixed, j)
-            if half_index == 0 and j == sp // 2 - 1:
-                pump_w(1, 2, quarters[1])
-        if half_index == 0:
-            pump_w(1, 2, quarters[2])
-        else:
-            for k in range(3, sp):
-                pump_w(1, k, quarters[0])
+            if j % 2:
+                advance()
 
         def next_rows(i, carry):
             within = pl.ds(pl.multiple_of(i * block, block), block)
@@ -548,27 +572,29 @@
             nrm[whole, :] = (v * scale * pre_ref[l + 1 : l + 2, :]).astype(jnp.bfloat16)
             return carry
 
-        lax.fori_loop(0, big // block, next_rows, 0)
+        middle = big // block // 2
+        lax.fori_loop(middle, big // block, next_rows, 0)
         if half_index == 0:
-            start(s < sp - 1, tail)
-            pump_w(1, 2, quarters[3])
-            pump_o(1, 2)
-        else:
-            for k in range(3, sp):
-                pump_w(1, k, quarters[1])
+            send_tail(1)
+        advance()
+        lax.fori_loop(0, middle, next_rows, 0)
+        advance()
 
     l = 1
     add_term(l, 0)
+    for one in far[6:7]:
+        one()
     add_term(l, 1)
-    for k in range(3, sp):
-        pump_w(1, k, quarters[2])
+    for one in far[7:8]:
+        one()
     x_phase(l, 1)
     for k in range(3, sp):
         add_term(l, k - 1)
-        pump_w(1, k, quarters[3])
+        for one in far[8:9]:
+            one()
         x_phase(l, k - 1)
-        c_phase(l, k - 2)
-        pump_o(1, k)
+        for one in far[9:10]:
+            one()
     tail_terms(l)
     last_term(l)
     for piece in reversed(range(tp)):
@@ -580,31 +606,59 @@
         def _():
             mlast[t] = raw
 
-        start(t != piece, lambda: copy(ms.at[at, :], mlast.at[t], a2s.at[0], a2r.at[0], tp=piece))
-    c_phase(l, sp - 2)
+        start(t != piece, lambda: copy(
+            ms.at[at, :], mlast.at[t], a2s.at[0], a2r.at[(piece // 2 + x) % 2], tp=piece))
+    for i in range(1, sp - 1):
+        c_phase(l, i)
+    copy(mlast.at[sibling], mlast.at[sibling], a2s.at[0], a2r.at[0], tp=sibling).wait_recv()
+    scaled_gain = 2 * ch
+
+    def side_rows(side):
+        return pl.ds(pl.multiple_of(side * scaled_gain, scaled_gain), scaled_gain)
+
+    def gained(side):
+        gain = mixg_ref[l : l + 1, side_rows(side)]
+        both_parts = jnp.concatenate([mlast[2 * side], mlast[2 * side + 1]], axis=1).astype(jnp.float32)
+        return both_parts, (both_parts * gain).astype(jnp.bfloat16)
+
+    def columns(i):
+        return pl.ds(pl.multiple_of(slice_at(i) * cols, cols), cols)
+
+    def product(mixed, i, side):
+        return jnp.dot(mixed, ow[l, slice_at(i), side_rows(side), :], preferred_element_type=jnp.float32)
+
+    mine, mine_mixed = gained(x)
+    for i in range(sp - 1):
+        if i > 0:
+            c_wait(l, i)
+        br[pl.ds(0, share), columns(i)] = product(mine_mixed, i, x)
     x_phase(l, sp - 1)
     c_phase(l, sp - 1)
-    others = mlast.at[pl.ds(0, tp - 1)]
-    copy(others, others, a2s.at[0], a2r.at[0], tp=sibling).wait_recv()
-    mixed = mix(l, lambda j: mlast[j])
+    drain()
+    yours_in = mlast.at[pl.ds(0, 2)]
+    copy(yours_in, yours_in, a2s.at[0], a2r.at[1], tp=across).wait_recv()
+    yours, yours_mixed = gained(1 - x)
+    total = jnp.sum(mine * mine + yours * yours, axis=-1, keepdims=True)
+    row_scale = lax.rsqrt(total * (1.0 / (tp * ch)) + EPS)
+    squares = jnp.zeros((share, 128), jnp.float32)
     for i in range(sp):
-        if i > 0:
+        if i < sp - 1:
+            sums = br[pl.ds(0, share), columns(i)] + product(yours_mixed, i, 1 - x)
+        else:
             c_wait(l, i)
-        project(l, mixed, slice_at(i))
-
-    def last_rows(i, carry):
-        at = pl.ds(pl.multiple_of(i * block, block), block)
-        b = br[at, :]
-        scale = lax.rsqrt(jnp.sum(b * b, axis=-1, keepdims=True) * (1.0 / width) + EPS)
-        out_ref[at, :] = (res[at, :] + b * scale * post_ref[l : l + 1, :]).astype(jnp.bfloat16)
-        return carry
-
-    lax.fori_loop(0, share // block, last_rows, 0)
-    drain()
+            sums = product(mine_mixed, i, x) + product(yours_mixed, i, 1 - x)
+        b = (sums * row_scale).astype(jnp.bfloat16).astype(jnp.float32)
+        br[pl.ds(0, share), columns(i)] = b
+        for lane in range(0, cols, 128):
+            squares = squares + b[:, lane : lane + 128] * b[:, lane : lane + 128]
+    scale = lax.rsqrt(jnp.sum(squares, axis=-1, keepdims=True) * (1.0 / width) + EPS)
+    out_ref[...] = (res[...] + br[pl.ds(0, share), :] * scale * post_ref[l : l + 1, :]).astype(jnp.bfloat16)
+    sent(ow.at[:, pl.ds(0, sp - 1), pl.ds(0, 4 * part), :], cs.at[0], tp=sibling)
+    sent(mlast.at[pl.ds(0, tp - 1)], a2s.at[0], tp=sibling)
 
 
 VPU_ROWS = 64
-PIECES = 4
+PIECES = 8
 VMEM_GRANT = 63 * 1024 * 1024
 
 
@@ -634,8 +688,8 @@
             pltpu.VMEM((8 + rows, ch), f32),
             pltpu.VMEM((rows, ch), bf),
             pltpu.VMEM((rows + 8, 3 * ch), f32),
-            pltpu.VMEM((16, ch), bf),
-            pltpu.VMEM((16, ch), bf),
+            pltpu.VMEM((layers, taps.shape[0] - 1, width), bf),
+            pltpu.VMEM((layers, taps.shape[0] - 1, width), bf),
             pltpu.VMEM((max(layers - 1, 1), tp, rows, ch), bf),
             pltpu.VMEM((rows, ch), bf),
             pltpu.VMEM((tp, share, ch), bf),
@@ -643,14 +697,14 @@
             pltpu.VMEM((share, width), f32),
             dma((layers,)), dma((layers,)), dma((1,)), dma((4,)),
             dma((2,)), dma((layers, sp - 1, PIECES)),
-            dma((layers, 2)), dma((layers, sp - 1)),
+            dma((layers, 2)), dma((layers, sp - 1, 2)),
             dma((1,)), dma((layers, sp - 1)),
             dma((layers,)), dma((layers, sp - 1)),
             dma((layers,)), dma((layers, sp - 1)),
             dma((1,)), dma((sp,)),
             dma((2,)), dma((2,)),
             dma((1,)), dma((tp,)), dma((2,)), dma((2,)),
-            dma((1,)), dma((1,)),
+            dma((1,)), dma((2,)),
         ],
         compiler_params=pltpu.CompilerParams(
             collective_id=0, has_side_effects=True, vmem_limit_bytes=VMEM_GRANT

time: 51.3 us -> 49.7 us (0.969)
  Pallas kernels: 50.4 us -> 48.8 us
    pallas_call x1, Pallas kernels: 50.4 us -> 48.8 us  [fused(): pl.pallas_call(functools.partial(fused_kernel, sizes), out_shape=pltpu.VM...]
where the time goes in v4:
time: 49.7 us; the launch traced here: 49.6 us
  Pallas kernels  48.8 us (98%)
  local copies, waits for them, and re-layouts  0.8 us (2%)
    pallas_call x1, Pallas kernels, fused(): pl.pallas_call(functools.partial(fused_kernel, sizes), out_shape=pltpu.VM...  48.8 us

profile of v4, /device:TPU:0, one launch (start us, length us, event | category | flops | bytes accessed | tf_op | source)
XLA Modules:
  0.0 49.6 jit_solution(5081432440390171018)
XLA Ops:
  0.0 48.8 %shard_map.91 = bf16[128,2048]{1,0:T(8,128)(2,1)S(1)} custom-call(bf16[512,2048]{1,0:T(8,128)(2,1)} %tok_hbm.1, bf16[2,512,128]{2,1,0:T(8,128)(2,1)} %gate_hbm.1, bf16[2,512,128]{2,1,0:T(8,128)(2,1)} %conv_hbm.1, bf16[2,512,128]{2,1,0:T(8,128)(2,1)} %value_hbm.1, bf16[2,512,512]{2,1,0:T(8,128)(2,1)} %outw_hbm.1, f32[3,2,512]{2,1,0:T(2,128)} %bitcast.1, ...), custom_call_target="tpu_custom_call" | custom-call | tf_op jit(solution)/shard_map/pallas_call | solution.py:674
  48.8 0.8 %copy.11 = bf16[128,2048]{1,0:T(8,128)(2,1)} copy(bf16[128,2048]{1,0:T(8,128)(2,1)S(1)} %shard_map.91) | data formatting | bytes 1048576
